TPU v7x, 128 devices: a whole 4x4x4 slice. The times are simulated.
128 devices in a mesh: sp: 16 (over z, x), tp: 8 (over y, core).
Axes of the slice: x: 4, y: 4, z: 4, core: 2. Of those that a mesh axis runs over, the one named last changes fastest.
Arguments:
- queries: bfloat16 [8192, 2048], P('sp', 'tp'), may hold values from -4.5 to 4.5
- keys: bfloat16 [8192, 2048], P('sp', 'tp'), may hold values from -4.5 to 4.5
- values: bfloat16 [8192, 2048], P('sp', 'tp'), may hold values from -6 to 6
- forget_logits: float32 [8192, 16], P('sp', 'tp'), may hold values from -1 to 20
- layer_input: bfloat16 [8192, 4096], P('sp', 'tp'), may hold values from -0.09375 to 0.09375
- out_grad: bfloat16 [8192, 2048], P('sp', 'tp'), may hold values from -6 to 6
Outputs:
- query_grad: float32 [8192, 2048], P('sp', 'tp')
- key_grad: float32 [8192, 2048], P('sp', 'tp')
- value_grad: float32 [8192, 2048], P('sp', 'tp')
- weight_grad: float32 [4096, 2048], P('sp', 'tp')
All inputs are finite; a program needn't handle non-finite values.
Results may differ from a plain program's by a relative error of at most 0.04.
Values may be sent and summed in bfloat16 or wider, within the bound.
A program may use at most 64 MiB of HBM per device.

v0:
```python
import jax
import jax.numpy as jnp
from jax import lax
from jax.experimental import pallas as pl
from jax.experimental.pallas import tpu as pltpu
from jax.sharding import PartitionSpec as P

HEAD = 128
LOG2E = 1.4426950408889634
SCALE = HEAD ** (-0.5)
LOW = jnp.bfloat16


def nt(a, b):
    return lax.dot_general(a, b, (((1,), (1,)), ((), ())), preferred_element_type=jnp.float32)


def nn(a, b):
    return lax.dot_general(a, b, (((1,), (0,)), ((), ())), preferred_element_type=jnp.float32)


def kernel_body(
    heads, parts, wide,
    q_in, g_in, k_in, v_in, gate_in, x_in,
    dq_out, dk_out, dv_out, w_out,
    kv, qg, gates, kt, vt, bias, sc, dk, dv, dq_stage, part_stage, red, fin, dq_got, kv_got,
    x_all, low, w_stage, w_red, w_fin, w_got,
    kv_recv, qg_recv, gate_recv, kv_send, qg_send, gate_send, relay_send,
    dq_send, dq_recv, part_send, red_recv, fin_send, fin_recv, local_sem,
    x_send, x_recv, w_send, w_recv, w_fin_send, w_fin_recv,
):
    blocks, _, rows, _ = kv.shape
    sub = qg.shape[2]
    span = w_out.shape[0]
    x_width = x_in.shape[1]
    column = lax.axis_index("tp")
    me = lax.axis_index("sp")
    head = me // parts
    part = lax.rem(me, parts)

    def remote(src, dst, send, recv, target):
        return pltpu.make_async_remote_copy(
            src_ref=src, dst_ref=dst, send_sem=send, recv_sem=recv, device_id={"sp": target}
        )

    barrier = pltpu.get_barrier_semaphore()
    for r in range(1, blocks):
        pl.semaphore_signal(barrier, inc=1, device_id={"sp": lax.rem(me + r, blocks)})
    for r in range(1, wide):
        pl.semaphore_signal(barrier, inc=1, device_id={"tp": lax.rem(column + r, wide)})
    pl.semaphore_wait(barrier, blocks + wide - 2)

    def lanes(h):
        return pl.ds(pl.multiple_of(h * HEAD, HEAD), HEAD)

    sources = ((k_in, v_in), (q_in, g_in))

    def place(r, c):
        return lax.rem(head + r, heads), lax.rem(part + c, parts)

    def kv_copy(r, i):
        h, _ = place(r, 0)
        return remote(
            sources[0][i].at[:, lanes(h)], kv.at[me, i], kv_send.at[r, i], kv_recv.at[me, i], h * parts + part
        )

    def relay_copy(r, c, i):
        h, other = place(r, c)
        j = h * parts + part
        src = sources[0][i].at[:, lanes(head)] if r == 0 else kv.at[j, i]
        return remote(src, kv.at[j, i], relay_send.at[r, c, i], kv_recv.at[j, i], head * parts + other)

    def q_source(r, c, i):
        h, other = place(r, c)
        begin = pl.multiple_of(lax.rem(other + me, parts) * sub, sub)
        return sources[1][i].at[pl.ds(begin, sub), lanes(h)]

    def q_copy(r, c, i):
        h, other = place(r, c)
        return remote(
            q_source(r, c, i), qg.at[me, i], qg_send.at[r, c, i], qg_recv.at[me, i], h * parts + other
        )

    def gate_copy(r, c):
        h, other = place(r, c)
        return remote(gate_in.at[h], gates.at[me], gate_send.at[r, c], gate_recv.at[me], h * parts + other)

    pairs = [(r, c) for r in range(heads) for c in range(parts) if (r, c) != (0, 0)]
    for r in range(1, heads):
        for i in range(2):
            kv_copy(r, i).start()
    for c in range(1, parts):
        for i in range(2):
            relay_copy(0, c, i).start()
    for r, c in pairs:
        gate_copy(r, c).start()
        for i in range(2):
            q_copy(r, c, i).start()
    own = [
        pltpu.make_async_copy(sources[0][i].at[:, lanes(head)], kv.at[me, i], local_sem.at[i]) for i in range(2)
    ]
    own += [pltpu.make_async_copy(q_source(0, 0, i), qg.at[me, i], local_sem.at[2 + i]) for i in range(2)]
    own += [pltpu.make_async_copy(gate_in.at[head], gates.at[me], local_sem.at[4])]
    own += [pltpu.make_async_copy(x_in, x_all.at[column], local_sem.at[5])]
    for copy in own:
        copy.start()

    def x_copy(r, source):
        return pltpu.make_async_remote_copy(
            src_ref=x_in,
            dst_ref=x_all.at[source],
            send_sem=x_send.at[r],
            recv_sem=x_recv.at[source],
            device_id={"tp": lax.rem(column + r, wide)},
        )

    for r in range(1, wide):
        x_copy(r, column).start()

    def kv_wait(j):
        for i in range(2):
            remote(kv.at[j, i], kv.at[j, i], kv_send.at[0, i], kv_recv.at[j, i], me).wait_recv()

    def turn(j):
        kt[j] = kv[j, 0].T
        vt[j] = kv[j, 1].T

    @pl.loop(0, blocks)
    def _(j):
        dk[j] = jnp.zeros((rows, HEAD), jnp.float32)
        dv[j] = jnp.zeros((rows, HEAD), jnp.float32)

    for copy in own:
        copy.wait()
    turn(me)
    for r in range(1, heads):
        j = place(r, 0)[0] * parts + part
        kv_wait(j)
        for c in range(1, parts):
            for i in range(2):
                relay_copy(r, c, i).start()
        turn(j)
    for r, c in pairs:
        h, other = place(r, c)
        j = h * parts + other
        if c:
            kv_wait(j)
            turn(j)
        for i in range(2):
            remote(qg.at[j, i], qg.at[j, i], qg_send.at[0, 0, i], qg_recv.at[j, i], me).wait_recv()
        remote(gates.at[j], gates.at[j], gate_send.at[0, 0], gate_recv.at[j], me).wait_recv()

    def prepare(j, base):
        row = gates[j, 0:1] + base
        bias[j] = jnp.broadcast_to(row, (HEAD, rows)).T
        return base + gates[j, 1:2]

    lax.fori_loop(0, blocks, prepare, jnp.zeros((1, rows), jnp.float32))

    def compute(b):
        q = qg[b, 0]
        g = qg[b, 1]
        offset = lax.rem(part + b, parts) * sub

        def score(j):
            return nt(kv[j, 0], q) * (SCALE * LOG2E) - bias[j][:, 0:1]

        def pass_a(j, top):
            s = score(j)
            sc[j] = s
            return jnp.maximum(top, jnp.max(s, axis=0, keepdims=True))

        top = lax.fori_loop(0, b, pass_a, jnp.full((1, sub), -1e30, jnp.float32))
        key_pos = lax.broadcasted_iota(jnp.int32, (rows, sub), 0)
        query_pos = lax.broadcasted_iota(jnp.int32, (rows, sub), 1) + offset
        s = jnp.where(key_pos <= query_pos, score(b), -1e30)
        sc[b] = s
        top = jnp.maximum(top, jnp.max(s, axis=0, keepdims=True))

        def pass_b(j, state):
            total, mixed = state
            w = jnp.exp2(sc[j] - top)
            sc[j] = w
            total = total + jnp.sum(w, axis=0, keepdims=True)
            return total, mixed + nn(vt[j], w.astype(LOW))

        total, mixed = lax.fori_loop(
            0, b + 1, pass_b, (jnp.zeros((1, sub), jnp.float32), jnp.zeros((HEAD, sub), jnp.float32))
        )
        attended = (mixed / total).astype(LOW).astype(jnp.float32)
        terms = jnp.sum(attended * g.astype(jnp.float32).T, axis=0, keepdims=True)
        inverse = 1.0 / total

        def pass_c(j, acc):
            prob = sc[j] * inverse
            ds = (prob * (nt(kv[j, 1], g) - terms)).astype(LOW)
            dv[j] += nn(prob.astype(LOW), g)
            dk[j] += nn(ds, q)
            return acc + nn(kt[j], ds)

        acc = lax.fori_loop(0, b + 1, pass_c, jnp.zeros((HEAD, sub), jnp.float32))
        dq_stage[b] = (acc * SCALE).T.astype(LOW)
        part_stage[b, 0] = (dk[b] * SCALE).astype(LOW)
        part_stage[b, 1] = dv[b].astype(LOW)

    def dq_copy(b):
        return remote(
            dq_stage.at[b], dq_got.at[head, lax.rem(part + b, parts)], dq_send.at[b], dq_recv.at[me], b
        )

    def part_copy(b):
        return remote(
            part_stage.at[b],
            red.at[b // parts, part],
            part_send.at[b],
            red_recv.at[b // parts, part],
            head * parts + lax.rem(b, parts),
        )

    def fin_copy(b):
        return remote(fin.at[b // parts], kv_got.at[head], fin_send.at[b // parts], fin_recv.at[head], b)

    def step(s, carry):
        b = blocks - 1 - s

        @pl.when(s < blocks)
        def _():
            compute(b)

        @pl.when((s >= 1) & (s < blocks + 1))
        def _():
            n = b + 1

            @pl.when(n == me)
            def _():
                dq_got[head, lax.rem(part + n, parts)] = dq_stage[n]

            @pl.when(n != me)
            def _():
                dq_copy(n).start()

            @pl.when(lax.rem(n, parts) != part)
            def _():
                part_copy(n).start()

        @pl.when((s >= 2) & (s < blocks + 2))
        def _():
            n = b + 2

            @pl.when(lax.rem(n, parts) == part)
            def _():
                slot = n // parts
                for c in range(1, parts):
                    other = lax.rem(part + c, parts)
                    remote(
                        red.at[slot, other], red.at[slot, other], part_send.at[0], red_recv.at[slot, other], me
                    ).wait_recv()
                for i in range(2):
                    value = dk[n] * SCALE if i == 0 else dv[n]
                    for c in range(1, parts):
                        value = value + red[slot, lax.rem(part + c, parts), i].astype(jnp.float32)
                    fin[slot, i] = value.astype(LOW)

        @pl.when(s >= 3)
        def _():
            n = b + 3

            @pl.when(lax.rem(n, parts) == part)
            def _():
                @pl.when(n == me)
                def _():
                    kv_got[head] = fin[n // parts]

                @pl.when(n != me)
                def _():
                    fin_copy(n).start()

        return carry

    lax.fori_loop(0, blocks + 3, step, 0)

    for r, c in pairs:
        h, other = place(r, c)
        slot = lax.rem(other + me, parts)
        remote(
            dq_got.at[h, slot], dq_got.at[h, slot], dq_send.at[0], dq_recv.at[h * parts + other], me
        ).wait_recv()
    for h in range(heads):
        for n in range(parts):
            low[n * sub : (n + 1) * sub, h * HEAD : (h + 1) * HEAD] = dq_got[h, n]
    for r in range(1, wide):
        x_copy(r, lax.rem(column + r, wide)).wait_recv()

    def term(c):
        begin = c * span
        x = x_all[begin // x_width, :, pl.ds(pl.multiple_of(lax.rem(begin, x_width), span), span)]
        return lax.dot_general(x, low[...], (((0,), (0,)), ((), ())), preferred_element_type=jnp.float32)

    def w_copy(r, c):
        h, other = place(r, c)
        return remote(
            w_stage.at[r, c], w_red.at[h, part], w_send.at[r, c], w_recv.at[h, part], head * parts + other
        )

    def w_fin_copy(r):
        h, _ = place(r, 0)
        return remote(w_fin.at[r], w_got.at[head], w_fin_send.at[r], w_fin_recv.at[head], h * parts + part)

    order = list(range(1, heads)) + [0]
    waiting = None
    for r in order:
        for c in range(1, parts):
            h, other = place(r, c)
            w_stage[r, c] = term(h * parts + other).astype(LOW)
            if waiting is not None:
                waiting.start()
            waiting = w_copy(r, c)
    dq_out[...] = low[...].astype(jnp.float32)
    if waiting is not None:
        waiting.start()
    waiting = None
    for r in order:
        h, _ = place(r, 0)
        w_out[...] = term(h * parts + part)
        if waiting is not None:
            waiting.start()
            waiting = None
        for c in range(1, parts):
            other = place(r, c)[1]
            remote(
                w_red.at[h, other], w_red.at[h, other], w_send.at[0, 0], w_recv.at[h, other], me
            ).wait_recv()
            w_out[...] += w_red[h, other].astype(jnp.float32)
        if r:
            w_fin[r] = w_out[...].astype(LOW)
            waiting = w_fin_copy(r)
    for r in range(1, heads):
        h, _ = place(r, 0)
        remote(kv_got.at[h], kv_got.at[h], fin_send.at[0], fin_recv.at[h], me).wait_recv()
    for h in range(heads):
        dk_out[:, h * HEAD : (h + 1) * HEAD] = kv_got[h, 0].astype(jnp.float32)
        dv_out[:, h * HEAD : (h + 1) * HEAD] = kv_got[h, 1].astype(jnp.float32)
    for r in range(1, heads):
        h, _ = place(r, 0)
        remote(w_got.at[h], w_got.at[h], w_fin_send.at[0], w_fin_recv.at[h], me).wait_recv()
        w_out[...] += w_got[h].astype(jnp.float32)
    for r in range(1, wide):
        x_copy(r, column).wait_send()
    for r in range(heads):
        for c in range(1, parts):
            w_copy(r, c).wait_send()
    for r in range(1, heads):
        w_fin_copy(r).wait_send()

    for r in range(1, heads):
        for i in range(2):
            kv_copy(r, i).wait_send()
    for r in range(heads):
        for c in range(1, parts):
            for i in range(2):
                relay_copy(r, c, i).wait_send()
    for r, c in pairs:
        gate_copy(r, c).wait_send()
        for i in range(2):
            q_copy(r, c, i).wait_send()

    @pl.loop(0, blocks)
    def _(b):
        @pl.when(b != me)
        def _():
            dq_copy(b).wait_send()

        @pl.when(lax.rem(b, parts) != part)
        def _():
            part_copy(b).wait_send()

        @pl.when((lax.rem(b, parts) == part) & (b != me))
        def _():
            fin_copy(b).wait_send()


def attention(heads, parts, wide, q, g, k, v, gate, x):
    blocks = heads * parts
    rows = k.shape[0]
    sub = rows // parts
    groups = blocks // parts
    vmem = pl.BlockSpec(memory_space=pltpu.VMEM)
    f32 = jnp.float32
    dma = pltpu.SemaphoreType.DMA
    cols = heads * HEAD
    span = x.shape[1] * wide // blocks
    grad = jax.ShapeDtypeStruct((rows, cols), f32)
    return pl.pallas_call(
        lambda *refs: kernel_body(heads, parts, wide, *refs),
        out_shape=(grad, grad, grad, jax.ShapeDtypeStruct((span, cols), f32)),
        in_specs=[vmem] * 6,
        out_specs=(vmem,) * 4,
        scratch_shapes=[
            pltpu.VMEM((blocks, 2, rows, HEAD), LOW),
            pltpu.VMEM((blocks, 2, sub, HEAD), LOW),
            pltpu.VMEM((blocks, 8, rows), f32),
            pltpu.VMEM((blocks, HEAD, rows), LOW),
            pltpu.VMEM((blocks, HEAD, rows), LOW),
            pltpu.VMEM((blocks, rows, HEAD), f32),
            pltpu.VMEM((blocks, rows, sub), f32),
            pltpu.VMEM((blocks, rows, HEAD), f32),
            pltpu.VMEM((blocks, rows, HEAD), f32),
            pltpu.VMEM((blocks, sub, HEAD), LOW),
            pltpu.VMEM((blocks, 2, rows, HEAD), LOW),
            pltpu.VMEM((groups, parts, 2, rows, HEAD), LOW),
            pltpu.VMEM((groups, 2, rows, HEAD), LOW),
            pltpu.VMEM((heads, parts, sub, HEAD), LOW),
            pltpu.VMEM((heads, 2, rows, HEAD), LOW),
            pltpu.VMEM((wide, rows, x.shape[1]), LOW),
            pltpu.VMEM((rows, cols), LOW),
            pltpu.VMEM((heads, parts, span, cols), LOW),
            pltpu.VMEM((heads, parts, span, cols), LOW),
            pltpu.VMEM((heads, span, cols), LOW),
            pltpu.VMEM((heads, span, cols), LOW),
            dma((blocks, 2)), dma((blocks, 2)), dma((blocks,)),
            dma((heads, 2)), dma((heads, parts, 2)), dma((heads, parts)), dma((heads, parts, 2)),
            dma((blocks,)), dma((blocks,)), dma((blocks,)), dma((groups, parts)),
            dma((groups,)), dma((heads,)), dma((6,)),
            dma((wide,)), dma((wide,)), dma((heads, parts)), dma((heads, parts)), dma((heads,)), dma((heads,)),
        ],
        compiler_params=pltpu.CompilerParams(
            vmem_limit_bytes=60 * 1024 * 1024, collective_id=0, has_side_effects=True
        ),
        cost_estimate=pl.CostEstimate(
            flops=12 * blocks * blocks * rows * sub * HEAD, bytes_accessed=1 << 22, transcendentals=0
        ),
        name="attention",
    )(q, g, k, v, gate, x)


def local(queries, keys, values, forget_logits, layer_input, out_grad):
    rows = queries.shape[0]
    heads = queries.shape[1] // HEAD
    parts = lax.axis_size("sp") // heads

    wide = lax.axis_size("tp")
    gates = jnp.cumsum(jax.nn.log_sigmoid(forget_logits), axis=0).T * LOG2E
    totals = jnp.broadcast_to(gates[:, None, rows - 1 :], (heads, 7, rows))
    gates = jnp.concatenate([gates[:, None], totals], axis=1)
    return attention(
        heads, parts, wide, queries, out_grad, keys, values, gates, layer_input
    )


def solution(mesh):
    spec = P("sp", "tp")
    return jax.shard_map(
        local, mesh=mesh, in_specs=(spec,) * 6, out_specs=(spec,) * 4, check_vma=False
    )
```

profile of v0, /device:TPU:0, one launch (start us, length us, event | category | flops | bytes accessed | tf_op | source)
XLA Modules:
  0.0 319.1 jit_solution(17399968717786114167)
XLA Ops:
  0.6 0.7 fusion.1
  1.4 0.6 reduce-window.6
  2.0 0.2 slice_reduce_fusion
  2.1 0.2 reduce-window.9
  2.3 0.1 add_multiply_fusion
  2.4 0.2 copy.12
  2.6 0.1 broadcast_in_dim.10
  2.6 0.6 pad_maximum_fusion.refs_4_
  3.3 310.9 %attention.1 = (f32[512,256]{1,0:T(8,128)}, f32[512,256]{1,0:T(8,128)}, f32[512,256]{1,0:T(8,128)}, f32[256,256]{1,0:T(8,128)}) custom-call(bf16[512,256]{1,0:T(8,128)(2,1)} %refs_0_.1, bf16[512,256]{1,0:T(8,128)(2,1)} %refs_1_.1, bf16[512,256]{1,0:T(8,128)(2,1)} %refs_2_.1, bf16[512,256]{1,0:T(8,128)(2,1)} %refs_3_.1, ...), custom_call_target="tpu_custom_call" | custom-call | flops 12884901888 | bytes 4194304 | tf_op jit(solution)/shard_map/attention/pallas_call | solution.py:393
  314.2 0.0 copy-start.1
  314.2 1.9 copy.17
  316.1 0.0 copy-done.1
  316.1 0.0 copy-start
  316.1 0.8 copy.18
  316.9 0.4 copy-done
  317.3 0.0 copy-start.2
  317.4 0.8 copy.19
  318.1 0.3 copy-done.2
  318.4 0.7 copy.20
  (2 shorter events, 0.0 us)
Async XLA Ops:
  314.2 1.9 copy-start.1
  316.1 1.2 copy-start
  317.3 1.1 copy-start.2
where the time goes:
time: 320 us; the launch traced here: 319 us
  Pallas kernels  311 us (97%)
  local copies, waits for them, and re-layouts  5.35 us (2%)
    pallas_call x1, Pallas kernels, attention(): pl.pallas_call(lambda *refs: kernel_body(heads, parts, wide, *refs), out_...  311 us

commit v1 on v0

v1 whole, which is shorter than its diff:
```python
import jax
import jax.numpy as jnp
from jax import lax
from jax.experimental import pallas as pl
from jax.experimental.pallas import tpu as pltpu
from jax.sharding import PartitionSpec as P

HEAD = 128
LOG2E = 1.4426950408889634
SCALE = HEAD ** (-0.5)
LOW = jnp.bfloat16
NX = 4
LAG = 2


def nt(a, b):
    return lax.dot_general(a, b, (((1,), (1,)), ((), ())), preferred_element_type=jnp.float32)


def nn(a, b):
    return lax.dot_general(a, b, (((1,), (0,)), ((), ())), preferred_element_type=jnp.float32)


def kernel_body(
    heads, wide,
    q_in, g_in, k_in, v_in, gate_in, x_in,
    dq_out, dk_out, dv_out, w_out,
    kv, qg, gates, kt, bias, wbuf, dpbuf, mrow, dk, dv, stat, stat_got,
    dq_stage, part_stage, red, fin, dq_got, kv_got,
    x_all, low, wa_stage, wb_stage, wa_red, wb_red, wa_own, wb_own, wa_fin, wb_fin, wa_got, wb_got,
    kv_recv, xs_send, col_send, x2_send, qg_recv, q_send, qf_send, gate_send, gate_recv, local_sem,
    stat_send, stat_recv, dq_send, dq_recv, part_send, red_recv, fin_send, fin_recv,
    x_send, xf_send, x_recv, wa_send, wb_send, wa_recv, wb_recv, wa_fsend, wb_fsend, wa_frecv, wb_frecv,
):
    blocks, _, hk, _ = kv.shape
    nx = NX
    nz = blocks // nx
    halves = nz // heads
    sub = qg.shape[2]
    tiles = blocks // 2
    span = w_out.shape[0]
    part_rows = span // 2
    x_width = x_in.shape[1]
    column = lax.axis_index("tp")
    me = lax.axis_index("sp")
    z = me // nx
    x = lax.rem(me, nx)
    head = z // halves
    half = lax.rem(z, halves)

    def at(zt, xt):
        return zt * nx + xt

    def near(r, c):
        return lax.rem(z + r, nz), lax.rem(x + c, nx)

    def remote(src, dst, send, recv, target):
        return pltpu.make_async_remote_copy(
            src_ref=src, dst_ref=dst, send_sem=send, recv_sem=recv, device_id={"sp": target}
        )

    def arrived(ref, recv):
        remote(ref, ref, dq_send.at[0], recv, me).wait_recv()

    barrier = pltpu.get_barrier_semaphore()
    for r in range(1, blocks):
        pl.semaphore_signal(barrier, inc=1, device_id={"sp": lax.rem(me + r, blocks)})
    for r in range(1, wide):
        pl.semaphore_signal(barrier, inc=1, device_id={"tp": lax.rem(column + r, wide)})
    pl.semaphore_wait(barrier, blocks + wide - 2)

    def lanes(h):
        return pl.ds(pl.multiple_of(h * HEAD, HEAD), HEAD)

    sent = []

    def go(copy):
        copy.start()
        sent.append(copy)

    kv_in = (k_in, v_in)
    qg_in = (q_in, g_in)

    def kv_source(i, zt):
        begin = pl.multiple_of(lax.rem(zt, halves) * hk, hk)
        return kv_in[i].at[pl.ds(begin, hk), lanes(zt // halves)]

    def q_source(i, zt, xt):
        begin = pl.multiple_of(xt * sub, sub)
        return qg_in[i].at[pl.ds(begin, sub), lanes(zt // halves)]

    for d, c in ((0, 1), (1, nx - 1)):
        for i in range(2):
            go(remote(kv_source(i, z), kv.at[me, i], xs_send.at[0, d, i], kv_recv.at[me, i], at(z, near(0, c)[1])))
    for r in (1, nz - 1, 2):
        zt = near(r, 0)[0]
        for i in range(2):
            go(remote(kv_source(i, zt), kv.at[me, i], col_send.at[r, i], kv_recv.at[me, i], at(zt, x)))

    across = nz - 1 - z
    partner = z + 1 - 2 * half

    def q_plane(r):
        return z if r == 0 else across

    for i in range(2):
        go(remote(q_source(i, z, x), qg.at[me, i], qf_send.at[0, 0, i], qg_recv.at[me, i], at(partner, x)))
    for r in range(heads):
        for c in range(nx):
            if (r, c) == (0, 0):
                continue
            zt, xt = q_plane(r), near(0, c)[1]
            for i in range(2):
                go(remote(q_source(i, zt, xt), qg.at[me, i], q_send.at[r, c, i], qg_recv.at[me, i], at(zt, xt)))
    for r in range(nz):
        for c in range(nx):
            if (r, c) == (0, 0):
                continue
            zt, xt = near(r, c)
            go(remote(gate_in.at[zt // halves], gates.at[me], gate_send.at[r, c], gate_recv.at[me], at(zt, xt)))

    def x_copy(src, source, target, send):
        return pltpu.make_async_remote_copy(
            src_ref=src, dst_ref=x_all.at[source], send_sem=send, recv_sem=x_recv.at[source], device_id={"tp": target}
        )

    core = lax.rem(column, 2)
    twin = column + 1 - 2 * core
    for r in range(1, wide // 2):
        go(x_copy(x_in, column, lax.rem(column + 2 * r, wide), x_send.at[r]))
    go(x_copy(x_in, column, twin, x_send.at[0]))

    own = [pltpu.make_async_copy(kv_source(i, z), kv.at[me, i], local_sem.at[i]) for i in range(2)]
    own += [pltpu.make_async_copy(q_source(i, z, x), qg.at[me, i], local_sem.at[2 + i]) for i in range(2)]
    own += [pltpu.make_async_copy(gate_in.at[head], gates.at[me], local_sem.at[4])]
    own += [pltpu.make_async_copy(x_in, x_all.at[column], local_sem.at[5])]
    for copy in own:
        copy.start()
    for copy in own:
        copy.wait()

    done = set()

    def kv_wait(r, c, i):
        if (r, c, i) in done:
            return
        done.add((r, c, i))
        j = at(*near(r, c))
        arrived(kv.at[j, i], kv_recv.at[j, i])

    def column_on(r):
        j = at(near(r, 0)[0], x)
        for i in range(2):
            kv_wait(r, 0, i)
            for d, c in ((0, 1), (1, nx - 1)):
                go(remote(kv.at[j, i], kv.at[j, i], xs_send.at[r, d, i], kv_recv.at[j, i], at(z, near(0, c)[1])))

    def second_on(r):
        for i, c in ((0, nx - 1), (1, 1)):
            kv_wait(r, c, i)
            j = at(*near(r, c))
            go(remote(kv.at[j, i], kv.at[j, i], x2_send.at[r, i], kv_recv.at[j, i], at(z, near(0, nx - c)[1])))

    def q_wait(j):
        for i in range(2):
            arrived(qg.at[j, i], qg_recv.at[j, i])

    def q_on(r, c):
        j = at(q_plane(r), near(0, c)[1])
        q_wait(j)
        for i in range(2):
            go(remote(qg.at[j, i], qg.at[j, i], qf_send.at[r, c, i], qg_recv.at[j, i], at(partner, x)))

    column_on(1)
    column_on(nz - 1)
    second_on(0)
    for c in range(1, nx):
        q_on(0, c)
    column_on(2)
    second_on(1)
    second_on(nz - 1)
    for c in range(nx):
        q_on(1, c)
    second_on(2)
    for plane in (partner, nz - 1 - partner):
        for c in range(nx):
            q_wait(at(plane, near(0, c)[1]))
    for r in range(nz):
        for c in range(nx):
            if (r, c) != (0, 0):
                j = at(*near(r, c))
                arrived(gates.at[j], gate_recv.at[j])

    def prepare(j, base):
        per = hk // HEAD
        table = gates[j]
        mine = table[0:per]
        for n in range(1, halves):
            mine = jnp.where(half == n, table[n * per : (n + 1) * per], mine)
        for n in range(per):
            row = mine[n : n + 1] + base
            bias[j, n * HEAD : (n + 1) * HEAD] = jnp.broadcast_to(row, (HEAD, HEAD)).T
        return base + table[halves * per : halves * per + 1]

    lax.fori_loop(0, blocks, prepare, jnp.zeros((1, HEAD), jnp.float32))
    for r in range(nz):
        for c in range(nx):
            if (r, c) != (0, 0):
                for i in range(2):
                    kv_wait(r, c, i)

    @pl.loop(0, tiles)
    def _(j):
        for n in range(2):
            kt[j, :, n * hk : (n + 1) * hk] = kv[2 * j + n, 0].T
        dk[j] = jnp.zeros((2 * hk, HEAD), jnp.float32)
        dv[j] = jnp.zeros((2 * hk, HEAD), jnp.float32)

    width = 2 * sub
    keys_wide = 2 * hk

    def forward(t):
        slot = lax.rem(t, 2)
        q = qg[pl.ds(2 * t, 2), 0].reshape(width, HEAD)
        g = qg[pl.ds(2 * t, 2), 1].reshape(width, HEAD)

        def block(j, state, mask):
            m, total, terms = state
            k = kv[pl.ds(2 * j, 2), 0].reshape(keys_wide, HEAD)
            v = kv[pl.ds(2 * j, 2), 1].reshape(keys_wide, HEAD)
            column_bias = bias[pl.ds(2 * j, 2)].reshape(keys_wide, HEAD)
            s = nt(k, q) * (SCALE * LOG2E) - jnp.concatenate([column_bias] * (width // HEAD), axis=1)
            if mask is not None:
                s = jnp.where(mask, s, -1e30)
            top = jnp.maximum(m, jnp.max(s, axis=0, keepdims=True))
            w = jnp.exp2(s - top)
            old = jnp.exp2(m - top)
            dp = nt(v, g)
            wbuf[slot, j] = w
            dpbuf[slot, j] = dp
            mrow[slot, j] = jnp.broadcast_to(top, (8, width))
            total = total * old + jnp.sum(w, axis=0, keepdims=True)
            terms = terms * old + jnp.sum(w * dp, axis=0, keepdims=True)
            return top, total, terms

        zero = jnp.zeros((1, width), jnp.float32)
        state = lax.fori_loop(
            0, t, lambda j, state: block(j, state, None), (jnp.full((1, width), -1e30, jnp.float32), zero, zero)
        )
        rows = halves * hk
        key_row = lax.broadcasted_iota(jnp.int32, (keys_wide, width), 0)
        query_row = lax.broadcasted_iota(jnp.int32, (keys_wide, width), 1)
        key_pos = jnp.where(key_row >= hk, key_row - hk + rows, key_row) + half * hk
        query_pos = jnp.where(query_row >= sub, query_row - sub + rows, query_row) + x * sub
        m, total, terms = block(t, state, key_pos <= query_pos)
        stat[t] = jnp.concatenate([m, total, terms, jnp.zeros((5, width), jnp.float32)], axis=0)

    def backward(t):
        slot = lax.rem(t, 2)
        q = qg[pl.ds(2 * t, 2), 0].reshape(width, HEAD)
        g = qg[pl.ds(2 * t, 2), 1].reshape(width, HEAD)
        arrived(stat_got.at[t], stat_recv.at[t])
        mine = stat[t]
        other = stat_got[t]
        top = jnp.maximum(mine[0:1], other[0:1])
        scale_mine = jnp.exp2(mine[0:1] - top)
        scale_other = jnp.exp2(other[0:1] - top)
        inverse = 1.0 / (mine[1:2] * scale_mine + other[1:2] * scale_other)
        terms = (mine[2:3] * scale_mine + other[2:3] * scale_other) * inverse

        def block(j, acc):
            factor = jnp.exp2(mrow[slot, j][0:1] - top) * inverse
            prob = wbuf[slot, j] * factor
            ds = (prob * (dpbuf[slot, j] - terms)).astype(LOW)
            dv[j] += nn(prob.astype(LOW), g)
            dk[j] += nn(ds, q)
            return acc + nn(kt[j], ds)

        acc = lax.fori_loop(0, t + 1, block, jnp.zeros((HEAD, width), jnp.float32))
        dq_t = (acc * SCALE).T.astype(LOW)
        for n in range(2):
            dq_stage[2 * t + n] = dq_t[n * sub : (n + 1) * sub]
            part_stage[2 * t + n, 0] = (dk[t, n * hk : (n + 1) * hk] * SCALE).astype(LOW)
            part_stage[2 * t + n, 1] = dv[t, n * hk : (n + 1) * hk].astype(LOW)

    def stat_copy(t):
        return remote(stat.at[t], stat_got.at[t], stat_send.at[t], stat_recv.at[t], at(partner, x))

    def dq_copy(n):
        return remote(dq_stage.at[n], dq_got.at[z, x], dq_send.at[n], dq_recv.at[me], n)

    def part_copy(n):
        return remote(
            part_stage.at[n], red.at[n // nx, x], part_send.at[n], red_recv.at[n // nx, x], at(z, lax.rem(n, nx))
        )

    def fin_copy(n):
        return remote(fin.at[n // nx], kv_got.at[z], fin_send.at[n // nx], fin_recv.at[z], n)

    def x_on(r):
        return x_copy(
            x_all.at[lax.rem(column + 2 * r, wide)], lax.rem(column + 2 * r, wide), twin, xf_send.at[r]
        )

    def step(s, carry):
        t = tiles - 1 - s

        @pl.when(s < tiles)
        def _():
            forward(t)

        @pl.when((s >= 2) & (s < tiles + 2))
        def _():
            for u in range(2):
                n = 2 * (t + 2) + u

                @pl.when(n == me)
                def _():
                    dq_got[z, x] = dq_stage[n]

                @pl.when(n != me)
                def _():
                    dq_copy(n).start()

                @pl.when(lax.rem(n, nx) != x)
                def _():
                    part_copy(n).start()

        @pl.when(s < tiles)
        def _():
            stat_copy(t).start()

        @pl.when((s >= 2 + LAG) & (s < tiles + 2 + LAG))
        def _():
            tile = t + 2 + LAG
            for u in range(2):
                n = 2 * tile + u

                @pl.when(lax.rem(n, nx) == x)
                def _():
                    zn = n // nx
                    for c in range(1, nx):
                        other = lax.rem(x + c, nx)
                        arrived(red.at[zn, other], red_recv.at[zn, other])
                    for i in range(2):
                        value = dk[tile, u * hk : (u + 1) * hk] * SCALE if i == 0 else dv[tile, u * hk : (u + 1) * hk]
                        for c in range(1, nx):
                            value = value + red[zn, lax.rem(x + c, nx), i].astype(jnp.float32)
                        fin[zn, i] = value.astype(LOW)

        @pl.when((s >= 1) & (s < tiles + 1))
        def _():
            backward(t + 1)

        @pl.when(s == 2)
        def _():
            for r in range(1, wide // 2):
                source = lax.rem(column + 2 * r, wide)
                pltpu.make_async_remote_copy(
                    src_ref=x_all.at[source], dst_ref=x_all.at[source], send_sem=xf_send.at[r],
                    recv_sem=x_recv.at[source], device_id={"tp": twin},
                ).wait_recv()
                x_on(r).start()

        @pl.when(s >= 3 + LAG)
        def _():
            for u in range(2):
                n = 2 * (t + 3 + LAG) + u

                @pl.when(lax.rem(n, nx) == x)
                def _():
                    @pl.when(n == me)
                    def _():
                        kv_got[z] = fin[n // nx]

                    @pl.when(n != me)
                    def _():
                        fin_copy(n).start()

        return carry

    lax.fori_loop(0, tiles + 3 + LAG, step, 0)

    for r in range(nz):
        for c in range(nx):
            if (r, c) != (0, 0):
                zs, xs = near(r, c)
                arrived(dq_got.at[zs, xs], dq_recv.at[at(zs, xs)])
    for h in range(heads):
        for n in range(nx):
            value = dq_got[h * halves, n].astype(jnp.float32)
            for m in range(1, halves):
                value = value + dq_got[h * halves + m, n].astype(jnp.float32)
            dq_out[n * sub : (n + 1) * sub, h * HEAD : (h + 1) * HEAD] = value
            low[n * sub : (n + 1) * sub, h * HEAD : (h + 1) * HEAD] = value.astype(LOW)
    for r in range(wide // 2):
        source = lax.rem(twin + 2 * r, wide)
        pltpu.make_async_remote_copy(
            src_ref=x_all.at[source], dst_ref=x_all.at[source], send_sem=x_send.at[0],
            recv_sem=x_recv.at[source], device_id={"tp": twin},
        ).wait_recv()

    def term(c):
        begin = c * span
        xs = x_all[begin // x_width, :, pl.ds(pl.multiple_of(lax.rem(begin, x_width), span), span)]
        return lax.dot_general(xs, low[...], (((0,), (0,)), ((), ())), preferred_element_type=jnp.float32)

    waiting = []

    def flush():
        for copy in waiting:
            go(copy)
        waiting.clear()

    order = [(r, c) for r in range(1, nz) for c in range(1, nx)]
    order += [(0, c) for c in range(1, nx)] + [(r, 0) for r in range(1, nz)] + [(0, 0)]
    for r, c in order:
        zt, xt = near(r, c)
        value = term(at(zt, xt))
        fresh = []
        if c:
            wa_stage[r, c] = value[:part_rows].astype(LOW)
            fresh.append(
                remote(wa_stage.at[r, c], wa_red.at[x, zt], wa_send.at[r, c], wa_recv.at[x, zt], at(z, xt))
            )
        else:
            wa_own[r] = value[:part_rows]
        if r:
            wb_stage[r, c] = value[part_rows:].astype(LOW)
            fresh.append(
                remote(wb_stage.at[r, c], wb_red.at[z, xt], wb_send.at[r, c], wb_recv.at[z, xt], at(zt, x))
            )
        else:
            wb_own[c] = value[part_rows:]
        flush()
        waiting.extend(fresh)
    flush()

    for n in list(range(1, nz)) + [0]:
        zt = near(n, 0)[0]
        value = wa_own[n]
        for c in range(1, nx):
            xs = near(0, c)[1]
            arrived(wa_red.at[xs, zt], wa_recv.at[xs, zt])
            value = value + wa_red[xs, zt].astype(jnp.float32)
        fresh = []
        if n:
            wa_fin[n] = value.astype(LOW)
            fresh.append(remote(wa_fin.at[n], wa_got.at[z], wa_fsend.at[n], wa_frecv.at[z], at(zt, x)))
        else:
            w_out[:part_rows] = value
        xt = near(0, n)[1]
        value = wb_own[n]
        for r in range(1, nz):
            zs = near(r, 0)[0]
            arrived(wb_red.at[zs, xt], wb_recv.at[zs, xt])
            value = value + wb_red[zs, xt].astype(jnp.float32)
        if n:
            wb_fin[n] = value.astype(LOW)
            fresh.append(remote(wb_fin.at[n], wb_got.at[x], wb_fsend.at[n], wb_frecv.at[x], at(z, xt)))
        else:
            w_out[part_rows:] = value
        flush()
        waiting.extend(fresh)
    flush()

    for r in range(1, nz):
        zs = near(r, 0)[0]
        arrived(kv_got.at[zs], fin_recv.at[zs])
    for h in range(heads):
        for m in range(halves):
            dk_out[m * hk : (m + 1) * hk, h * HEAD : (h + 1) * HEAD] = kv_got[h * halves + m, 0].astype(jnp.float32)
            dv_out[m * hk : (m + 1) * hk, h * HEAD : (h + 1) * HEAD] = kv_got[h * halves + m, 1].astype(jnp.float32)
    for n in range(1, nz):
        zs = near(n, 0)[0]
        arrived(wa_got.at[zs], wa_frecv.at[zs])
        w_out[:part_rows] += wa_got[zs].astype(jnp.float32)
        xs = near(0, n)[1]
        arrived(wb_got.at[xs], wb_frecv.at[xs])
        w_out[part_rows:] += wb_got[xs].astype(jnp.float32)

    for copy in sent:
        copy.wait_send()
    for r in range(1, wide // 2):
        x_on(r).wait_send()

    @pl.loop(0, tiles)
    def _(t):
        stat_copy(t).wait_send()

    @pl.loop(0, blocks)
    def _(n):
        @pl.when(n != me)
        def _():
            dq_copy(n).wait_send()

        @pl.when(lax.rem(n, nx) != x)
        def _():
            part_copy(n).wait_send()

        @pl.when((lax.rem(n, nx) == x) & (n != me))
        def _():
            fin_copy(n).wait_send()


def attention(blocks, wide, q, g, k, v, gate, x):
    rows, cols = k.shape
    heads = cols // HEAD
    nx = NX
    nz = blocks // nx
    halves = nz // heads
    hk = rows // halves
    sub = rows // nx
    tiles = blocks // 2
    vmem = pl.BlockSpec(memory_space=pltpu.VMEM)
    f32 = jnp.float32
    dma = pltpu.SemaphoreType.DMA
    span = x.shape[1] * wide // blocks
    part = span // 2
    grad = jax.ShapeDtypeStruct((rows, cols), f32)
    return pl.pallas_call(
        lambda *refs: kernel_body(heads, wide, *refs),
        out_shape=(grad, grad, grad, jax.ShapeDtypeStruct((span, cols), f32)),
        in_specs=[vmem] * 6,
        out_specs=(vmem,) * 4,
        scratch_shapes=[
            pltpu.VMEM((blocks, 2, hk, HEAD), LOW),
            pltpu.VMEM((blocks, 2, sub, HEAD), LOW),
            pltpu.VMEM((blocks, 8, HEAD), f32),
            pltpu.VMEM((tiles, HEAD, 2 * hk), LOW),
            pltpu.VMEM((blocks, hk, HEAD), f32),
            pltpu.VMEM((2, tiles, 2 * hk, 2 * sub), f32),
            pltpu.VMEM((2, tiles, 2 * hk, 2 * sub), f32),
            pltpu.VMEM((2, tiles, 8, 2 * sub), f32),
            pltpu.VMEM((tiles, 2 * hk, HEAD), f32),
            pltpu.VMEM((tiles, 2 * hk, HEAD), f32),
            pltpu.VMEM((tiles, 8, 2 * sub), f32),
            pltpu.VMEM((tiles, 8, 2 * sub), f32),
            pltpu.VMEM((blocks, sub, HEAD), LOW),
            pltpu.VMEM((blocks, 2, hk, HEAD), LOW),
            pltpu.VMEM((nz, nx, 2, hk, HEAD), LOW),
            pltpu.VMEM((nz, 2, hk, HEAD), LOW),
            pltpu.VMEM((nz, nx, sub, HEAD), LOW),
            pltpu.VMEM((nz, 2, hk, HEAD), LOW),
            pltpu.VMEM((wide, rows, x.shape[1]), LOW),
            pltpu.VMEM((rows, cols), LOW),
            pltpu.VMEM((nz, nx, part, cols), LOW),
            pltpu.VMEM((nz, nx, part, cols), LOW),
            pltpu.VMEM((nx, nz, part, cols), LOW),
            pltpu.VMEM((nz, nx, part, cols), LOW),
            pltpu.VMEM((nz, part, cols), f32),
            pltpu.VMEM((nx, part, cols), f32),
            pltpu.VMEM((nz, part, cols), LOW),
            pltpu.VMEM((nx, part, cols), LOW),
            pltpu.VMEM((nz, part, cols), LOW),
            pltpu.VMEM((nx, part, cols), LOW),
            dma((blocks, 2)), dma((nz, 2, 2)), dma((nz, 2)), dma((nz, 2)), dma((blocks, 2)), dma((heads, nx, 2)),
            dma((heads, nx, 2)), dma((nz, nx)), dma((blocks,)), dma((6,)),
            dma((tiles,)), dma((tiles,)), dma((blocks,)), dma((blocks,)), dma((blocks,)), dma((nz, nx)),
            dma((nz,)), dma((nz,)),
            dma((wide // 2,)), dma((wide // 2,)), dma((wide,)),
            dma((nz, nx)), dma((nz, nx)), dma((nx, nz)), dma((nz, nx)),
            dma((nz,)), dma((nx,)), dma((nz,)), dma((nx,)),
        ],
        compiler_params=pltpu.CompilerParams(
            vmem_limit_bytes=62 * 1024 * 1024, collective_id=0, has_side_effects=True
        ),
        cost_estimate=pl.CostEstimate(
            flops=10 * blocks * blocks * rows * sub * HEAD, bytes_accessed=1 << 22, transcendentals=0
        ),
        name="attention",
    )(q, g, k, v, gate, x)


def local(queries, keys, values, forget_logits, layer_input, out_grad):
    rows = queries.shape[0]
    heads = queries.shape[1] // HEAD
    blocks = lax.axis_size("sp")
    wide = lax.axis_size("tp")
    gates = jnp.cumsum(jax.nn.log_sigmoid(forget_logits), axis=0).T * LOG2E
    totals = jnp.broadcast_to(gates[:, rows - 1 :, None], (heads, 8 - rows // HEAD, HEAD))
    gates = jnp.concatenate([gates.reshape(heads, rows // HEAD, HEAD), totals], axis=1)
    return attention(blocks, wide, queries, out_grad, keys, values, gates, layer_input)


def solution(mesh):
    spec = P("sp", "tp")
    return jax.shard_map(
        local, mesh=mesh, in_specs=(spec,) * 6, out_specs=(spec,) * 4, check_vma=False
    )
```

time: 320 us -> 118 us (0.37)
  Pallas kernels: 311 us -> 110 us
    pallas_call x1, Pallas kernels: 311 us -> 110 us  [attention(): pl.pallas_call(lambda *refs: kernel_body(heads, wide, *refs), out_shape=(...]
where the time goes in v1:
time: 118 us
  Pallas kernels  110 us (93%)
  local copies, waits for them, and re-layouts  5.35 us (5%)
  other arithmetic  2.2 us (2%)
    pallas_call x1, Pallas kernels, attention(): pl.pallas_call(lambda *refs: kernel_body(heads, wide, *refs), out_shape=(...  110 us
    unnamed x10, local copies, waits for them, and re-layouts  4.95 us

profile of v1, /device:TPU:0, one launch (start us, length us, event | category | flops | bytes accessed | tf_op | source)
XLA Modules:
  0.0 117.8 jit_solution(17665122592423421019)
XLA Ops:
  0.6 0.7 fusion.1
  1.4 0.6 reduce-window.6
  2.0 0.2 slice_reduce_fusion
  2.1 0.2 reduce-window.9
  2.3 0.1 add_multiply_fusion
  2.4 0.2 copy.12
  2.6 0.1 broadcast_in_dim.9
  2.6 0.6 pad_maximum_fusion.refs_4_
  3.3 109.5 %attention.1 = (f32[512,256]{1,0:T(8,128)}, f32[512,256]{1,0:T(8,128)}, f32[512,256]{1,0:T(8,128)}, f32[256,256]{1,0:T(8,128)}) custom-call(bf16[512,256]{1,0:T(8,128)(2,1)} %refs_0_.1, bf16[512,256]{1,0:T(8,128)(2,1)} %refs_1_.1, bf16[512,256]{1,0:T(8,128)(2,1)} %refs_2_.1, bf16[512,256]{1,0:T(8,128)(2,1)} %refs_3_.1, ...), custom_call_target="tpu_custom_call" | custom-call | flops 21474836480 | bytes 4194304 | tf_op jit(solution)/shard_map/attention/pallas_call | solution.py:521
  112.8 0.0 copy-start.1
  112.8 1.9 %copy.17 = f32[512,256]{1,0:T(8,128)} copy(f32[512,256]{1,0:T(8,128)} %get-tuple-element.8) | data formatting | bytes 1048576
  114.7 0.0 copy-done.1
  114.7 0.0 copy-start
  114.7 0.8 copy.18
  115.5 0.4 copy-done
  116.0 0.0 copy-start.2
  116.0 0.8 copy.19
  116.8 0.3 copy-done.2
  117.1 0.7 copy.20
  (2 shorter events, 0.0 us)
Async XLA Ops:
  112.8 1.9 %copy-start.1 = (f32[512,256]{1,0:T(8,128)S(1)}, f32[512,256]{1,0:T(8,128)}, u32[]{:S(2)}) copy-start(f32[512,256]{1,0:T(8,128)} %get-tuple-element.9) | copy-start | bytes 1572868
  114.7 1.2 %copy-start = (f32[512,256]{1,0:T(8,128)S(1)}, f32[512,256]{1,0:T(8,128)}, u32[]{:S(2)}) copy-start(f32[512,256]{1,0:T(8,128)} %get-tuple-element.10) | copy-start | bytes 1572868
  116.0 1.1 copy-start.2

commit v2 on v1

--- a/solution.py
+++ b/solution.py
@@ -10,7 +10,6 @@
 SCALE = HEAD ** (-0.5)
 LOW = jnp.bfloat16
 NX = 4
-LAG = 2
 
 
 def nt(a, b):
@@ -26,10 +25,10 @@
     q_in, g_in, k_in, v_in, gate_in, x_in,
     dq_out, dk_out, dv_out, w_out,
     kv, qg, gates, kt, bias, wbuf, dpbuf, mrow, dk, dv, stat, stat_got,
-    dq_stage, part_stage, red, fin, dq_got, kv_got,
+    dq_stage, part_stage, mid, red, fin, dq_got, kv_got,
     x_all, low, wa_stage, wb_stage, wa_red, wb_red, wa_own, wb_own, wa_fin, wb_fin, wa_got, wb_got,
     kv_recv, xs_send, col_send, x2_send, qg_recv, q_send, qf_send, gate_send, gate_recv, local_sem,
-    stat_send, stat_recv, dq_send, dq_recv, part_send, red_recv, fin_send, fin_recv,
+    stat_send, stat_recv, dq_send, dq_recv, part_send, mid_recv, red_recv, fin_send, fin_recv,
     x_send, xf_send, x_recv, wa_send, wb_send, wa_recv, wb_recv, wa_fsend, wb_fsend, wa_frecv, wb_frecv,
 ):
     blocks, _, hk, _ = kv.shape
@@ -89,6 +88,13 @@
         begin = pl.multiple_of(xt * sub, sub)
         return qg_in[i].at[pl.ds(begin, sub), lanes(zt // halves)]
 
+    for r in range(nz):
+        for c in range(nx):
+            if (r, c) == (0, 0):
+                continue
+            zt, xt = near(r, c)
+            go(remote(gate_in.at[zt // halves], gates.at[me], gate_send.at[r, c], gate_recv.at[me], at(zt, xt)))
+
     for d, c in ((0, 1), (1, nx - 1)):
         for i in range(2):
             go(remote(kv_source(i, z), kv.at[me, i], xs_send.at[0, d, i], kv_recv.at[me, i], at(z, near(0, c)[1])))
@@ -112,12 +118,6 @@
             zt, xt = q_plane(r), near(0, c)[1]
             for i in range(2):
                 go(remote(q_source(i, zt, xt), qg.at[me, i], q_send.at[r, c, i], qg_recv.at[me, i], at(zt, xt)))
-    for r in range(nz):
-        for c in range(nx):
-            if (r, c) == (0, 0):
-                continue
-            zt, xt = near(r, c)
-            go(remote(gate_in.at[zt // halves], gates.at[me], gate_send.at[r, c], gate_recv.at[me], at(zt, xt)))
 
     def x_copy(src, source, target, send):
         return pltpu.make_async_remote_copy(
@@ -138,6 +138,11 @@
         copy.start()
     for copy in own:
         copy.wait()
+
+    @pl.loop(0, tiles)
+    def _(j):
+        dk[j] = jnp.zeros((2 * hk, HEAD), jnp.float32)
+        dv[j] = jnp.zeros((2 * hk, HEAD), jnp.float32)
 
     done = set()
 
@@ -182,9 +187,6 @@
     for c in range(nx):
         q_on(1, c)
     second_on(2)
-    for plane in (partner, nz - 1 - partner):
-        for c in range(nx):
-            q_wait(at(plane, near(0, c)[1]))
     for r in range(nz):
         for c in range(nx):
             if (r, c) != (0, 0):
@@ -203,6 +205,9 @@
         return base + table[halves * per : halves * per + 1]
 
     lax.fori_loop(0, blocks, prepare, jnp.zeros((1, HEAD), jnp.float32))
+    for plane in (partner, nz - 1 - partner):
+        for c in range(nx):
+            q_wait(at(plane, near(0, c)[1]))
     for r in range(nz):
         for c in range(nx):
             if (r, c) != (0, 0):
@@ -213,8 +218,6 @@
     def _(j):
         for n in range(2):
             kt[j, :, n * hk : (n + 1) * hk] = kv[2 * j + n, 0].T
-        dk[j] = jnp.zeros((2 * hk, HEAD), jnp.float32)
-        dv[j] = jnp.zeros((2 * hk, HEAD), jnp.float32)
 
     width = 2 * sub
     keys_wide = 2 * hk
@@ -276,12 +279,14 @@
             dk[j] += nn(ds, q)
             return acc + nn(kt[j], ds)
 
-        acc = lax.fori_loop(0, t + 1, block, jnp.zeros((HEAD, width), jnp.float32))
+        acc = block(t, jnp.zeros((HEAD, width), jnp.float32))
+        for n in range(2):
+            part_stage[2 * t + n, 0] = (dk[t, n * hk : (n + 1) * hk] * SCALE).astype(LOW)
+            part_stage[2 * t + n, 1] = dv[t, n * hk : (n + 1) * hk].astype(LOW)
+        acc = lax.fori_loop(0, t, block, acc)
         dq_t = (acc * SCALE).T.astype(LOW)
         for n in range(2):
             dq_stage[2 * t + n] = dq_t[n * sub : (n + 1) * sub]
-            part_stage[2 * t + n, 0] = (dk[t, n * hk : (n + 1) * hk] * SCALE).astype(LOW)
-            part_stage[2 * t + n, 1] = dv[t, n * hk : (n + 1) * hk].astype(LOW)
 
     def stat_copy(t):
         return remote(stat.at[t], stat_got.at[t], stat_send.at[t], stat_recv.at[t], at(partner, x))
@@ -289,10 +294,98 @@
     def dq_copy(n):
         return remote(dq_stage.at[n], dq_got.at[z, x], dq_send.at[n], dq_recv.at[me], n)
 
-    def part_copy(n):
+    def away(n):
+        return lax.rem(lax.rem(n, nx) + nx - x, nx)
+
+    def opposite_copy(n, i):
+        xt = lax.rem(x + (1 if i == 0 else nx - 1), nx)
+        return remote(part_stage.at[n, i], mid.at[n // nx, i], part_send.at[n, i], mid_recv.at[n // nx, i], at(z, xt))
+
+    def near_copy(n, side, i):
         return remote(
-            part_stage.at[n], red.at[n // nx, x], part_send.at[n], red_recv.at[n // nx, x], at(z, lax.rem(n, nx))
+            part_stage.at[n, i], red.at[n // nx, side, i], part_send.at[n, i], red_recv.at[n // nx, side, i],
+            at(z, lax.rem(n, nx)),
         )
+
+    def first_sends(tile):
+        for u in range(2):
+            n = 2 * tile + u
+
+            @pl.when(away(n) == 2)
+            def _():
+                opposite_copy(n, 0).start()
+                opposite_copy(n, 1).start()
+
+            @pl.when(away(n) == 1)
+            def _():
+                near_copy(n, 0, 1).start()
+
+            @pl.when(away(n) == nx - 1)
+            def _():
+                near_copy(n, 1, 0).start()
+
+    def add_on_way(tile):
+        for u in range(2):
+            n = 2 * tile + u
+            zn = n // nx
+            for i, d in ((0, 1), (1, nx - 1)):
+
+                @pl.when(away(n) == d)
+                def _():
+                    arrived(mid.at[zn, i], mid_recv.at[zn, i])
+                    value = dk[tile, u * hk : (u + 1) * hk] * SCALE if i == 0 else dv[tile, u * hk : (u + 1) * hk]
+                    part_stage[n, i] = (value + mid[zn, i].astype(jnp.float32)).astype(LOW)
+
+    def second_sends(tile):
+        for u in range(2):
+            n = 2 * tile + u
+
+            @pl.when(away(n) == 1)
+            def _():
+                near_copy(n, 0, 0).start()
+
+            @pl.when(away(n) == nx - 1)
+            def _():
+                near_copy(n, 1, 1).start()
+
+    def reduce(tile):
+        for u in range(2):
+            n = 2 * tile + u
+
+            @pl.when(away(n) == 0)
+            def _():
+                zn = n // nx
+                for i in range(2):
+                    for side in range(2):
+                        arrived(red.at[zn, side, i], red_recv.at[zn, side, i])
+                    value = dk[tile, u * hk : (u + 1) * hk] * SCALE if i == 0 else dv[tile, u * hk : (u + 1) * hk]
+                    for side in range(2):
+                        value = value + red[zn, side, i].astype(jnp.float32)
+                    fin[zn, i] = value.astype(LOW)
+
+    def fin_sends(tile):
+        for u in range(2):
+            n = 2 * tile + u
+
+            @pl.when((away(n) == 0) & (n == me))
+            def _():
+                kv_got[z] = fin[n // nx]
+
+            @pl.when((away(n) == 0) & (n != me))
+            def _():
+                fin_copy(n).start()
+
+    def dq_sends(tile):
+        for u in range(2):
+            n = 2 * tile + u
+
+            @pl.when(n == me)
+            def _():
+                dq_got[z, x] = dq_stage[n]
+
+            @pl.when(n != me)
+            def _():
+                dq_copy(n).start()
 
     def fin_copy(n):
         return remote(fin.at[n // nx], kv_got.at[z], fin_send.at[n // nx], fin_recv.at[z], n)
@@ -305,52 +398,18 @@
     def step(s, carry):
         t = tiles - 1 - s
 
-        @pl.when(s < tiles)
-        def _():
-            forward(t)
-
-        @pl.when((s >= 2) & (s < tiles + 2))
-        def _():
-            for u in range(2):
-                n = 2 * (t + 2) + u
-
-                @pl.when(n == me)
-                def _():
-                    dq_got[z, x] = dq_stage[n]
-
-                @pl.when(n != me)
-                def _():
-                    dq_copy(n).start()
-
-                @pl.when(lax.rem(n, nx) != x)
-                def _():
-                    part_copy(n).start()
-
-        @pl.when(s < tiles)
-        def _():
-            stat_copy(t).start()
-
-        @pl.when((s >= 2 + LAG) & (s < tiles + 2 + LAG))
-        def _():
-            tile = t + 2 + LAG
-            for u in range(2):
-                n = 2 * tile + u
-
-                @pl.when(lax.rem(n, nx) == x)
-                def _():
-                    zn = n // nx
-                    for c in range(1, nx):
-                        other = lax.rem(x + c, nx)
-                        arrived(red.at[zn, other], red_recv.at[zn, other])
-                    for i in range(2):
-                        value = dk[tile, u * hk : (u + 1) * hk] * SCALE if i == 0 else dv[tile, u * hk : (u + 1) * hk]
-                        for c in range(1, nx):
-                            value = value + red[zn, lax.rem(x + c, nx), i].astype(jnp.float32)
-                        fin[zn, i] = value.astype(LOW)
-
-        @pl.when((s >= 1) & (s < tiles + 1))
-        def _():
-            backward(t + 1)
+        def stage(offset, work):
+            pl.when((t + offset >= 0) & (t + offset < tiles))(lambda: work(t + offset))
+
+        stage(0, forward)
+        stage(2, dq_sends)
+        stage(3, second_sends)
+        stage(5, fin_sends)
+        stage(0, lambda tile: stat_copy(tile).start())
+        stage(1, backward)
+        stage(1, first_sends)
+        stage(2, add_on_way)
+        stage(4, reduce)
 
         @pl.when(s == 2)
         def _():
@@ -362,24 +421,11 @@
                 ).wait_recv()
                 x_on(r).start()
 
-        @pl.when(s >= 3 + LAG)
-        def _():
-            for u in range(2):
-                n = 2 * (t + 3 + LAG) + u
-
-                @pl.when(lax.rem(n, nx) == x)
-                def _():
-                    @pl.when(n == me)
-                    def _():
-                        kv_got[z] = fin[n // nx]
-
-                    @pl.when(n != me)
-                    def _():
-                        fin_copy(n).start()
-
         return carry
 
-    lax.fori_loop(0, tiles + 3 + LAG, step, 0)
+    lax.fori_loop(0, tiles + 2, step, 0)
+    second_sends(0)
+    fin_sends(2)
 
     for r in range(nz):
         for c in range(nx):
@@ -393,6 +439,7 @@
                 value = value + dq_got[h * halves + m, n].astype(jnp.float32)
             dq_out[n * sub : (n + 1) * sub, h * HEAD : (h + 1) * HEAD] = value
             low[n * sub : (n + 1) * sub, h * HEAD : (h + 1) * HEAD] = value.astype(LOW)
+    reduce(1)
     for r in range(wide // 2):
         source = lax.rem(twin + 2 * r, wide)
         pltpu.make_async_remote_copy(
@@ -435,6 +482,8 @@
         flush()
         waiting.extend(fresh)
     flush()
+    fin_sends(1)
+    reduce(0)
 
     for n in list(range(1, nz)) + [0]:
         zt = near(n, 0)[0]
@@ -464,6 +513,7 @@
         waiting.extend(fresh)
     flush()
 
+    fin_sends(0)
     for r in range(1, nz):
         zs = near(r, 0)[0]
         arrived(kv_got.at[zs], fin_recv.at[zs])
@@ -494,11 +544,19 @@
         def _():
             dq_copy(n).wait_send()
 
-        @pl.when(lax.rem(n, nx) != x)
+        @pl.when(away(n) == 2)
         def _():
-            part_copy(n).wait_send()
-
-        @pl.when((lax.rem(n, nx) == x) & (n != me))
+            for i in range(2):
+                opposite_copy(n, i).wait_send()
+
+        for d, side in ((1, 0), (nx - 1, 1)):
+
+            @pl.when(away(n) == d)
+            def _():
+                for i in range(2):
+                    near_copy(n, side, i).wait_send()
+
+        @pl.when((away(n) == 0) & (n != me))
         def _():
             fin_copy(n).wait_send()
 
@@ -538,7 +596,8 @@
             pltpu.VMEM((tiles, 8, 2 * sub), f32),
             pltpu.VMEM((blocks, sub, HEAD), LOW),
             pltpu.VMEM((blocks, 2, hk, HEAD), LOW),
-            pltpu.VMEM((nz, nx, 2, hk, HEAD), LOW),
+            pltpu.VMEM((nz, 2, hk, HEAD), LOW),
+            pltpu.VMEM((nz, 2, 2, hk, HEAD), LOW),
             pltpu.VMEM((nz, 2, hk, HEAD), LOW),
             pltpu.VMEM((nz, nx, sub, HEAD), LOW),
             pltpu.VMEM((nz, 2, hk, HEAD), LOW),
@@ -556,7 +615,7 @@
             pltpu.VMEM((nx, part, cols), LOW),
             dma((blocks, 2)), dma((nz, 2, 2)), dma((nz, 2)), dma((nz, 2)), dma((blocks, 2)), dma((heads, nx, 2)),
             dma((heads, nx, 2)), dma((nz, nx)), dma((blocks,)), dma((6,)),
-            dma((tiles,)), dma((tiles,)), dma((blocks,)), dma((blocks,)), dma((blocks,)), dma((nz, nx)),
+            dma((tiles,)), dma((tiles,)), dma((blocks,)), dma((blocks,)), dma((blocks, 2)), dma((nz, 2)), dma((nz, 2, 2)),
             dma((nz,)), dma((nz,)),
             dma((wide // 2,)), dma((wide // 2,)), dma((wide,)),
             dma((nz, nx)), dma((nz, nx)), dma((nx, nz)), dma((nz, nx)),

time: 118 us -> 114 us (0.966)
  Pallas kernels: 110 us -> 105 us
    pallas_call x1, Pallas kernels: 110 us -> 105 us  [attention(): pl.pallas_call(lambda *refs: kernel_body(heads, wide, *refs), out_shape=(...]
where the time goes in v2:
time: 114 us
  Pallas kernels  105 us (92%)
  local copies, waits for them, and re-layouts  5.35 us (5%)
  other arithmetic  2.2 us (2%)
    pallas_call x1, Pallas kernels, attention(): pl.pallas_call(lambda *refs: kernel_body(heads, wide, *refs), out_shape=(...  105 us
    unnamed x10, local copies, waits for them, and re-layouts  4.95 us

profile of v2, /device:TPU:0, one launch (start us, length us, event | category | flops | bytes accessed | tf_op | source)
XLA Modules:
  0.0 113.5 jit_solution(2649007934099462850)
XLA Ops:
  0.6 0.7 fusion.1
  1.4 0.6 reduce-window.6
  2.0 0.2 slice_reduce_fusion
  2.1 0.2 reduce-window.9
  2.3 0.1 add_multiply_fusion
  2.4 0.2 copy.12
  2.6 0.1 broadcast_in_dim.9
  2.6 0.6 pad_maximum_fusion.refs_4_
  3.3 105.3 %attention.1 = (f32[512,256]{1,0:T(8,128)}, f32[512,256]{1,0:T(8,128)}, f32[512,256]{1,0:T(8,128)}, f32[256,256]{1,0:T(8,128)}) custom-call(bf16[512,256]{1,0:T(8,128)(2,1)} %refs_0_.1, bf16[512,256]{1,0:T(8,128)(2,1)} %refs_1_.1, bf16[512,256]{1,0:T(8,128)(2,1)} %refs_2_.1, bf16[512,256]{1,0:T(8,128)(2,1)} %refs_3_.1, ...), custom_call_target="tpu_custom_call" | custom-call | flops 21474836480 | bytes 4194304 | tf_op jit(solution)/shard_map/attention/pallas_call | solution.py:579
  108.5 0.0 copy-start.1
  108.6 1.9 %copy.17 = f32[512,256]{1,0:T(8,128)} copy(f32[512,256]{1,0:T(8,128)} %get-tuple-element.8) | data formatting | bytes 1048576
  110.5 0.0 copy-done.1
  110.5 0.0 copy-start
  110.5 0.8 copy.18
  111.3 0.4 copy-done
  111.7 0.0 copy-start.2
  111.7 0.8 copy.19
  112.5 0.3 copy-done.2
  112.8 0.7 copy.20
  (2 shorter events, 0.0 us)
Async XLA Ops:
  108.5 1.9 %copy-start.1 = (f32[512,256]{1,0:T(8,128)S(1)}, f32[512,256]{1,0:T(8,128)}, u32[]{:S(2)}) copy-start(f32[512,256]{1,0:T(8,128)} %get-tuple-element.9) | copy-start | bytes 1572868
  110.5 1.2 %copy-start = (f32[512,256]{1,0:T(8,128)S(1)}, f32[512,256]{1,0:T(8,128)}, u32[]{:S(2)}) copy-start(f32[512,256]{1,0:T(8,128)} %get-tuple-element.10) | copy-start | bytes 1572868
  111.7 1.1 copy-start.2

commit v3 on v2

--- a/solution.py
+++ b/solution.py
@@ -22,12 +22,12 @@
 
 def kernel_body(
     heads, wide,
-    q_in, g_in, k_in, v_in, gate_in, x_in,
-    dq_out, dk_out, dv_out, w_out,
-    kv, qg, gates, kt, bias, wbuf, dpbuf, mrow, dk, dv, stat, stat_got,
+    q_hbm, g_hbm, k_hbm, v_hbm, logits_hbm, x_hbm,
+    low_out, kv_out, w_out,
+    q_in, g_in, k_in, v_in, logits, gate_in, w_sum, kv, qg, gates, kt, bias, wbuf, dpbuf, mrow, dk, dv, stat, stat_got,
     dq_stage, part_stage, mid, red, fin, dq_got, kv_got,
     x_all, low, wa_stage, wb_stage, wa_red, wb_red, wa_own, wb_own, wa_fin, wb_fin, wa_got, wb_got,
-    kv_recv, xs_send, col_send, x2_send, qg_recv, q_send, qf_send, gate_send, gate_recv, local_sem,
+    in_sem, out_sem, kv_recv, xs_send, col_send, x2_send, qg_recv, q_send, qf_send, gate_send, gate_recv, local_sem,
     stat_send, stat_recv, dq_send, dq_recv, part_send, mid_recv, red_recv, fin_send, fin_recv,
     x_send, xf_send, x_recv, wa_send, wb_send, wa_recv, wb_recv, wa_fsend, wb_fsend, wa_frecv, wb_frecv,
 ):
@@ -39,7 +39,7 @@
     tiles = blocks // 2
     span = w_out.shape[0]
     part_rows = span // 2
-    x_width = x_in.shape[1]
+    x_width = x_hbm.shape[1]
     column = lax.axis_index("tp")
     me = lax.axis_index("sp")
     z = me // nx
@@ -66,7 +66,6 @@
         pl.semaphore_signal(barrier, inc=1, device_id={"sp": lax.rem(me + r, blocks)})
     for r in range(1, wide):
         pl.semaphore_signal(barrier, inc=1, device_id={"tp": lax.rem(column + r, wide)})
-    pl.semaphore_wait(barrier, blocks + wide - 2)
 
     def lanes(h):
         return pl.ds(pl.multiple_of(h * HEAD, HEAD), HEAD)
@@ -87,6 +86,49 @@
     def q_source(i, zt, xt):
         begin = pl.multiple_of(xt * sub, sub)
         return qg_in[i].at[pl.ds(begin, sub), lanes(zt // halves)]
+
+    loads = [
+        pltpu.make_async_copy(src, dst, in_sem.at[n])
+        for n, (src, dst) in enumerate(
+            ((logits_hbm, logits), (k_hbm, k_in), (v_hbm, v_in), (q_hbm, q_in), (g_hbm, g_in), (x_hbm, x_all.at[column]))
+        )
+    ]
+    for copy in loads:
+        copy.start()
+
+    @pl.loop(0, tiles)
+    def _(j):
+        dk[j] = jnp.zeros((2 * hk, HEAD), jnp.float32)
+        dv[j] = jnp.zeros((2 * hk, HEAD), jnp.float32)
+
+    loads[0].wait()
+    chunks = logits.shape[1] // HEAD
+    raw = jnp.concatenate(
+        [logits[h : h + 1, u * HEAD : (u + 1) * HEAD] for h in range(heads) for u in range(chunks)], axis=0
+    )
+    logs = (jnp.minimum(raw, 0.0) - jnp.log1p(jnp.exp(-jnp.abs(raw)))) * LOG2E
+    upto = lax.broadcasted_iota(jnp.int32, (HEAD, HEAD), 0) <= lax.broadcasted_iota(jnp.int32, (HEAD, HEAD), 1)
+    sums = jnp.dot(
+        logs, upto.astype(jnp.float32), precision=lax.Precision.HIGHEST, preferred_element_type=jnp.float32
+    )
+    for h in range(heads):
+        base = jnp.zeros((1, HEAD), jnp.float32)
+        for u in range(chunks):
+            line = sums[h * chunks + u : h * chunks + u + 1]
+            gate_in[h, u : u + 1] = line + base
+            base = base + jnp.broadcast_to(line[:, HEAD - 1 :], (1, HEAD))
+        gate_in[h, chunks:] = jnp.broadcast_to(base, (gate_in.shape[1] - chunks, HEAD))
+
+    for copy in loads[1:]:
+        copy.wait()
+    own = [pltpu.make_async_copy(kv_source(i, z), kv.at[me, i], local_sem.at[i]) for i in range(2)]
+    own += [pltpu.make_async_copy(q_source(i, z, x), qg.at[me, i], local_sem.at[2 + i]) for i in range(2)]
+    own += [pltpu.make_async_copy(gate_in.at[head], gates.at[me], local_sem.at[4])]
+    for copy in own:
+        copy.start()
+    for copy in own:
+        copy.wait()
+    pl.semaphore_wait(barrier, blocks + wide - 2)
 
     for r in range(nz):
         for c in range(nx):
@@ -127,22 +169,8 @@
     core = lax.rem(column, 2)
     twin = column + 1 - 2 * core
     for r in range(1, wide // 2):
-        go(x_copy(x_in, column, lax.rem(column + 2 * r, wide), x_send.at[r]))
-    go(x_copy(x_in, column, twin, x_send.at[0]))
-
-    own = [pltpu.make_async_copy(kv_source(i, z), kv.at[me, i], local_sem.at[i]) for i in range(2)]
-    own += [pltpu.make_async_copy(q_source(i, z, x), qg.at[me, i], local_sem.at[2 + i]) for i in range(2)]
-    own += [pltpu.make_async_copy(gate_in.at[head], gates.at[me], local_sem.at[4])]
-    own += [pltpu.make_async_copy(x_in, x_all.at[column], local_sem.at[5])]
-    for copy in own:
-        copy.start()
-    for copy in own:
-        copy.wait()
-
-    @pl.loop(0, tiles)
-    def _(j):
-        dk[j] = jnp.zeros((2 * hk, HEAD), jnp.float32)
-        dv[j] = jnp.zeros((2 * hk, HEAD), jnp.float32)
+        go(x_copy(x_all.at[column], column, lax.rem(column + 2 * r, wide), x_send.at[r]))
+    go(x_copy(x_all.at[column], column, twin, x_send.at[0]))
 
     done = set()
 
@@ -437,8 +465,8 @@
             value = dq_got[h * halves, n].astype(jnp.float32)
             for m in range(1, halves):
                 value = value + dq_got[h * halves + m, n].astype(jnp.float32)
-            dq_out[n * sub : (n + 1) * sub, h * HEAD : (h + 1) * HEAD] = value
             low[n * sub : (n + 1) * sub, h * HEAD : (h + 1) * HEAD] = value.astype(LOW)
+    low_copy = pltpu.make_async_copy(low, low_out, out_sem.at[0])
     reduce(1)
     for r in range(wide // 2):
         source = lax.rem(twin + 2 * r, wide)
@@ -482,6 +510,7 @@
         flush()
         waiting.extend(fresh)
     flush()
+    low_copy.start()
     fin_sends(1)
     reduce(0)
 
@@ -497,7 +526,7 @@
             wa_fin[n] = value.astype(LOW)
             fresh.append(remote(wa_fin.at[n], wa_got.at[z], wa_fsend.at[n], wa_frecv.at[z], at(zt, x)))
         else:
-            w_out[:part_rows] = value
+            w_sum[:part_rows] = value
         xt = near(0, n)[1]
         value = wb_own[n]
         for r in range(1, nz):
@@ -508,7 +537,7 @@
             wb_fin[n] = value.astype(LOW)
             fresh.append(remote(wb_fin.at[n], wb_got.at[x], wb_fsend.at[n], wb_frecv.at[x], at(z, xt)))
         else:
-            w_out[part_rows:] = value
+            w_sum[part_rows:] = value
         flush()
         waiting.extend(fresh)
     flush()
@@ -517,18 +546,20 @@
     for r in range(1, nz):
         zs = near(r, 0)[0]
         arrived(kv_got.at[zs], fin_recv.at[zs])
-    for h in range(heads):
-        for m in range(halves):
-            dk_out[m * hk : (m + 1) * hk, h * HEAD : (h + 1) * HEAD] = kv_got[h * halves + m, 0].astype(jnp.float32)
-            dv_out[m * hk : (m + 1) * hk, h * HEAD : (h + 1) * HEAD] = kv_got[h * halves + m, 1].astype(jnp.float32)
+    kv_copy = pltpu.make_async_copy(kv_got, kv_out, out_sem.at[1])
+    kv_copy.start()
     for n in range(1, nz):
         zs = near(n, 0)[0]
         arrived(wa_got.at[zs], wa_frecv.at[zs])
-        w_out[:part_rows] += wa_got[zs].astype(jnp.float32)
+        w_sum[:part_rows] += wa_got[zs].astype(jnp.float32)
         xs = near(0, n)[1]
         arrived(wb_got.at[xs], wb_frecv.at[xs])
-        w_out[part_rows:] += wb_got[xs].astype(jnp.float32)
-
+        w_sum[part_rows:] += wb_got[xs].astype(jnp.float32)
+
+    w_copy = pltpu.make_async_copy(w_sum, w_out, out_sem.at[2])
+    w_copy.start()
+    low_copy.wait()
+    kv_copy.wait()
     for copy in sent:
         copy.wait_send()
     for r in range(1, wide // 2):
@@ -560,8 +591,10 @@
         def _():
             fin_copy(n).wait_send()
 
-
-def attention(blocks, wide, q, g, k, v, gate, x):
+    w_copy.wait()
+
+
+def attention(blocks, wide, q, g, k, v, logits, x):
     rows, cols = k.shape
     heads = cols // HEAD
     nx = NX
@@ -570,18 +603,28 @@
     hk = rows // halves
     sub = rows // nx
     tiles = blocks // 2
-    vmem = pl.BlockSpec(memory_space=pltpu.VMEM)
+    anywhere = pl.BlockSpec(memory_space=pl.ANY)
     f32 = jnp.float32
     dma = pltpu.SemaphoreType.DMA
     span = x.shape[1] * wide // blocks
     part = span // 2
-    grad = jax.ShapeDtypeStruct((rows, cols), f32)
     return pl.pallas_call(
         lambda *refs: kernel_body(heads, wide, *refs),
-        out_shape=(grad, grad, grad, jax.ShapeDtypeStruct((span, cols), f32)),
-        in_specs=[vmem] * 6,
-        out_specs=(vmem,) * 4,
+        out_shape=(
+            jax.ShapeDtypeStruct((rows, cols), LOW),
+            jax.ShapeDtypeStruct((nz, 2, hk, HEAD), LOW),
+            jax.ShapeDtypeStruct((span, cols), f32),
+        ),
+        in_specs=[anywhere] * 6,
+        out_specs=(anywhere,) * 3,
         scratch_shapes=[
+            pltpu.VMEM((rows, cols), LOW),
+            pltpu.VMEM((rows, cols), LOW),
+            pltpu.VMEM((rows, cols), LOW),
+            pltpu.VMEM((rows, cols), LOW),
+            pltpu.VMEM((heads, rows), f32),
+            pltpu.VMEM((heads, 8, HEAD), f32),
+            pltpu.VMEM((span, cols), f32),
             pltpu.VMEM((blocks, 2, hk, HEAD), LOW),
             pltpu.VMEM((blocks, 2, sub, HEAD), LOW),
             pltpu.VMEM((blocks, 8, HEAD), f32),
@@ -613,6 +656,7 @@
             pltpu.VMEM((nx, part, cols), LOW),
             pltpu.VMEM((nz, part, cols), LOW),
             pltpu.VMEM((nx, part, cols), LOW),
+            dma((6,)), dma((3,)),
             dma((blocks, 2)), dma((nz, 2, 2)), dma((nz, 2)), dma((nz, 2)), dma((blocks, 2)), dma((heads, nx, 2)),
             dma((heads, nx, 2)), dma((nz, nx)), dma((blocks,)), dma((6,)),
             dma((tiles,)), dma((tiles,)), dma((blocks,)), dma((blocks,)), dma((blocks, 2)), dma((nz, 2)), dma((nz, 2, 2)),
@@ -628,18 +672,64 @@
             flops=10 * blocks * blocks * rows * sub * HEAD, bytes_accessed=1 << 22, transcendentals=0
         ),
         name="attention",
-    )(q, g, k, v, gate, x)
+    )(q, g, k, v, logits, x)
+
+
+def finish_body(
+    heads, low_hbm, kv_hbm, w_hbm, dq_out, dk_out, dv_out, w_out, low, kv, w, dq, dk, dv, in_sem, out_sem
+):
+    halves = kv.shape[0] // heads
+    hk = kv.shape[2]
+    loads = [
+        pltpu.make_async_copy(src, dst, in_sem.at[n])
+        for n, (src, dst) in enumerate(((low_hbm, low), (kv_hbm, kv), (w_hbm, w)))
+    ]
+    for copy in loads:
+        copy.start()
+    stores = [
+        pltpu.make_async_copy(src, dst, out_sem.at[n])
+        for n, (src, dst) in enumerate(((dq, dq_out), (dk, dk_out), (dv, dv_out), (w, w_out)))
+    ]
+    loads[0].wait()
+    dq[...] = low[...].astype(jnp.float32)
+    stores[0].start()
+    loads[1].wait()
+    for i, grad in enumerate((dk, dv)):
+        for h in range(heads):
+            for m in range(halves):
+                grad[m * hk : (m + 1) * hk, h * HEAD : (h + 1) * HEAD] = kv[h * halves + m, i].astype(jnp.float32)
+        stores[1 + i].start()
+    loads[2].wait()
+    stores[3].start()
+    for copy in stores:
+        copy.wait()
+
+
+def finish(heads, low, kv, w):
+    anywhere = pl.BlockSpec(memory_space=pl.ANY)
+    f32 = jnp.float32
+    grad = jax.ShapeDtypeStruct(low.shape, f32)
+    return pl.pallas_call(
+        lambda *refs: finish_body(heads, *refs),
+        out_shape=(grad, grad, grad, jax.ShapeDtypeStruct(w.shape, f32)),
+        in_specs=[anywhere] * 3,
+        out_specs=(anywhere,) * 4,
+        scratch_shapes=[
+            pltpu.VMEM(low.shape, LOW), pltpu.VMEM(kv.shape, LOW), pltpu.VMEM(w.shape, f32),
+            pltpu.VMEM(low.shape, f32), pltpu.VMEM(low.shape, f32), pltpu.VMEM(low.shape, f32),
+            pltpu.SemaphoreType.DMA((3,)), pltpu.SemaphoreType.DMA((4,)),
+        ],
+        compiler_params=pltpu.CompilerParams(vmem_limit_bytes=62 * 1024 * 1024),
+        name="finish",
+    )(low, kv, w)
 
 
 def local(queries, keys, values, forget_logits, layer_input, out_grad):
-    rows = queries.shape[0]
     heads = queries.shape[1] // HEAD
     blocks = lax.axis_size("sp")
     wide = lax.axis_size("tp")
-    gates = jnp.cumsum(jax.nn.log_sigmoid(forget_logits), axis=0).T * LOG2E
-    totals = jnp.broadcast_to(gates[:, rows - 1 :, None], (heads, 8 - rows // HEAD, HEAD))
-    gates = jnp.concatenate([gates.reshape(heads, rows // HEAD, HEAD), totals], axis=1)
-    return attention(blocks, wide, queries, out_grad, keys, values, gates, layer_input)
+    pieces = attention(blocks, wide, queries, out_grad, keys, values, forget_logits.T, layer_input)
+    return finish(heads, *pieces)
 
 
 def solution(mesh):

time: 114 us -> 107 us (0.939)
  local copies, waits for them, and re-layouts: 5.35 us -> 0 us
  other arithmetic: 2.2 us -> 0 us
    unnamed x10 -> x0, local copies, waits for them, and re-layouts: 4.95 us -> none
    pallas_call x0 -> x1, Pallas kernels: none -> 2.27 us  [finish(): pl.pallas_call(lambda *refs: finish_body(heads, *refs), out_shape=(grad,...]
    pallas_call x1, Pallas kernels: 105 us -> 104 us  [attention(): pl.pallas_call(lambda *refs: kernel_body(heads, wide, *refs), out_shape=(...]
where the time goes in v3:
time: 107 us
  Pallas kernels  106 us (99%)
    pallas_call x1, Pallas kernels, attention(): pl.pallas_call(lambda *refs: kernel_body(heads, wide, *refs), out_shape=(...  104 us
    pallas_call x1, Pallas kernels, finish(): pl.pallas_call(lambda *refs: finish_body(heads, *refs), out_shape=(grad,...  2.27 us

profile of v3, /device:TPU:0, one launch (start us, length us, event | category | flops | bytes accessed | tf_op | source)
XLA Modules:
  0.0 106.6 jit_solution(4384544504850827687)
XLA Ops:
  0.6 103.7 %attention.1 = (bf16[512,256]{1,0:T(8,128)(2,1)}, bf16[4,2,256,128]{3,2,1,0:T(8,128)(2,1)}, f32[256,256]{1,0:T(8,128)}) custom-call(bf16[512,256]{1,0:T(8,128)(2,1)} %refs_0_.1, bf16[512,256]{1,0:T(8,128)(2,1)} %refs_1_.1, bf16[512,256]{1,0:T(8,128)(2,1)} %refs_2_.1, bf16[512,256]{1,0:T(8,128)(2,1)} %refs_3_.1, f32[2,512]{1,0:T(2,128)} %bitcast.1, ...), custom_call_target="tpu_custom_call" | custom-call | flops 21474836480 | bytes 4194304 | tf_op jit(solution)/shard_map/attention/pallas_call | solution.py:611
  104.3 2.3 %finish.1 = (f32[512,256]{1,0:T(8,128)}, f32[512,256]{1,0:T(8,128)}, f32[512,256]{1,0:T(8,128)}, f32[256,256]{1,0:T(8,128)}) custom-call(bf16[512,256]{1,0:T(8,128)(2,1)} %get-tuple-element.7.refs_0_, bf16[4,2,256,128]{3,2,1,0:T(8,128)(2,1)} %get-tuple-element.8.refs_1_, f32[256,256]{1,0:T(8,128)} %get-tuple-element.9.refs_2_), custom_call_target="tpu_custom_call" | custom-call | tf_op jit(solution)/shard_map/finish/pallas_call | solution.py:712

commit v4 on v3

--- a/solution.py
+++ b/solution.py
@@ -24,7 +24,7 @@
     heads, wide,
     q_hbm, g_hbm, k_hbm, v_hbm, logits_hbm, x_hbm,
     low_out, kv_out, w_out,
-    q_in, g_in, k_in, v_in, logits, gate_in, w_sum, kv, qg, gates, kt, bias, wbuf, dpbuf, mrow, dk, dv, stat, stat_got,
+    q_in, g_in, k_in, v_in, logits, gate_in, w_sum, kv, qg, gates, kt, bias, wbuf, mrow, dk, dv, stat, stat_got,
     dq_stage, part_stage, mid, red, fin, dq_got, kv_got,
     x_all, low, wa_stage, wb_stage, wa_red, wb_red, wa_own, wb_own, wa_fin, wb_fin, wa_got, wb_got,
     in_sem, out_sem, kv_recv, xs_send, col_send, x2_send, qg_recv, q_send, qf_send, gate_send, gate_recv, local_sem,
@@ -96,10 +96,15 @@
     for copy in loads:
         copy.start()
 
+    width = 2 * sub
+    keys_wide = 2 * hk
+    line = lax.broadcasted_iota(jnp.int32, (8, width), 0)
+
     @pl.loop(0, tiles)
     def _(j):
-        dk[j] = jnp.zeros((2 * hk, HEAD), jnp.float32)
-        dv[j] = jnp.zeros((2 * hk, HEAD), jnp.float32)
+        dk[j] = jnp.zeros((keys_wide, HEAD), jnp.float32)
+        dv[j] = jnp.zeros((keys_wide, HEAD), jnp.float32)
+        stat[j] = jnp.where(line == 0, -1e30, 0.0)
 
     loads[0].wait()
     chunks = logits.shape[1] // HEAD
@@ -137,9 +142,6 @@
             zt, xt = near(r, c)
             go(remote(gate_in.at[zt // halves], gates.at[me], gate_send.at[r, c], gate_recv.at[me], at(zt, xt)))
 
-    for d, c in ((0, 1), (1, nx - 1)):
-        for i in range(2):
-            go(remote(kv_source(i, z), kv.at[me, i], xs_send.at[0, d, i], kv_recv.at[me, i], at(z, near(0, c)[1])))
     for r in (1, nz - 1, 2):
         zt = near(r, 0)[0]
         for i in range(2):
@@ -172,27 +174,32 @@
         go(x_copy(x_all.at[column], column, lax.rem(column + 2 * r, wide), x_send.at[r]))
     go(x_copy(x_all.at[column], column, twin, x_send.at[0]))
 
-    done = set()
-
-    def kv_wait(r, c, i):
-        if (r, c, i) in done:
-            return
-        done.add((r, c, i))
-        j = at(*near(r, c))
+    def kv_arrived(j, i):
         arrived(kv.at[j, i], kv_recv.at[j, i])
 
-    def column_on(r):
-        j = at(near(r, 0)[0], x)
+    def round_copy(p, c, i):
+        j = at(p, x)
+        return remote(kv.at[j, i], kv.at[j, i], xs_send.at[p, c // 2, i], kv_recv.at[j, i], at(z, near(0, c)[1]))
+
+    def onward_copy(p, i):
+        c = nx - 1 if i == 0 else 1
+        j = at(p, near(0, c)[1])
+        return remote(kv.at[j, i], kv.at[j, i], x2_send.at[p, i], kv_recv.at[j, i], at(z, near(0, nx - c)[1]))
+
+    def column_on(p):
+        @pl.when(z != p)
+        def _():
+            for i in range(2):
+                kv_arrived(at(p, x), i)
+
         for i in range(2):
-            kv_wait(r, 0, i)
-            for d, c in ((0, 1), (1, nx - 1)):
-                go(remote(kv.at[j, i], kv.at[j, i], xs_send.at[r, d, i], kv_recv.at[j, i], at(z, near(0, c)[1])))
-
-    def second_on(r):
+            for c in (1, nx - 1):
+                round_copy(p, c, i).start()
+
+    def second_on(p):
         for i, c in ((0, nx - 1), (1, 1)):
-            kv_wait(r, c, i)
-            j = at(*near(r, c))
-            go(remote(kv.at[j, i], kv.at[j, i], x2_send.at[r, i], kv_recv.at[j, i], at(z, near(0, nx - c)[1])))
+            kv_arrived(at(p, near(0, c)[1]), i)
+            onward_copy(p, i).start()
 
     def q_wait(j):
         for i in range(2):
@@ -204,17 +211,16 @@
         for i in range(2):
             go(remote(qg.at[j, i], qg.at[j, i], qf_send.at[r, c, i], qg_recv.at[j, i], at(partner, x)))
 
+    column_on(0)
     column_on(1)
-    column_on(nz - 1)
-    second_on(0)
     for c in range(1, nx):
         q_on(0, c)
+    second_on(0)
     column_on(2)
-    second_on(1)
-    second_on(nz - 1)
+    column_on(3)
     for c in range(nx):
         q_on(1, c)
-    second_on(2)
+    second_on(1)
     for r in range(nz):
         for c in range(nx):
             if (r, c) != (0, 0):
@@ -236,60 +242,72 @@
     for plane in (partner, nz - 1 - partner):
         for c in range(nx):
             q_wait(at(plane, near(0, c)[1]))
-    for r in range(nz):
-        for c in range(nx):
-            if (r, c) != (0, 0):
-                for i in range(2):
-                    kv_wait(r, c, i)
-
-    @pl.loop(0, tiles)
-    def _(j):
+
+    rows = halves * hk
+    key_row = lax.broadcasted_iota(jnp.int32, (keys_wide, width), 0)
+    query_row = lax.broadcasted_iota(jnp.int32, (keys_wide, width), 1)
+    key_pos = jnp.where(key_row >= hk, key_row - hk + rows, key_row) + half * hk
+    query_pos = jnp.where(query_row >= sub, query_row - sub + rows, query_row) + x * sub
+
+    def pair(i, j):
+        return kv[pl.ds(2 * j, 2), i].reshape(keys_wide, HEAD)
+
+    def queries(i, t):
+        return qg[pl.ds(2 * t, 2), i].reshape(width, HEAD)
+
+    def place(t, j):
+        return t * (t + 1) // 2 + j
+
+    def scores(t, j, masked):
+        state = stat[t]
+        m, total, terms = state[0:1], state[1:2], state[2:3]
+        column_bias = bias[pl.ds(2 * j, 2)].reshape(keys_wide, HEAD)
+        s = nt(pair(0, j), queries(0, t)) * (SCALE * LOG2E) - jnp.concatenate([column_bias] * (width // HEAD), axis=1)
+        if masked:
+            s = jnp.where(key_pos <= query_pos, s, -1e30)
+        top = jnp.maximum(m, jnp.max(s, axis=0, keepdims=True))
+        w = jnp.exp2(s - top)
+        old = jnp.exp2(m - top)
+        dp = nt(pair(1, j), queries(1, t))
+        wbuf[place(t, j)] = w
+        mrow[place(t, j)] = jnp.broadcast_to(top, (8, width))
+        total = total * old + jnp.sum(w, axis=0, keepdims=True)
+        terms = terms * old + jnp.sum(w * dp, axis=0, keepdims=True)
+        stat[t] = jnp.concatenate([top, total, terms, jnp.zeros((5, width), jnp.float32)], axis=0)
+
+    def forward(j, carry):
+        for u in range(2):
+            b = 2 * j + u
+            d = lax.rem(lax.rem(b, nx) + nx - x, nx)
+
+            @pl.when((d == 1) | (d == 2))
+            def _():
+                kv_arrived(b, 0)
+
+            @pl.when((d == nx - 1) | (d == 2))
+            def _():
+                kv_arrived(b, 1)
+
         for n in range(2):
             kt[j, :, n * hk : (n + 1) * hk] = kv[2 * j + n, 0].T
-
-    width = 2 * sub
-    keys_wide = 2 * hk
-
-    def forward(t):
-        slot = lax.rem(t, 2)
-        q = qg[pl.ds(2 * t, 2), 0].reshape(width, HEAD)
-        g = qg[pl.ds(2 * t, 2), 1].reshape(width, HEAD)
-
-        def block(j, state, mask):
-            m, total, terms = state
-            k = kv[pl.ds(2 * j, 2), 0].reshape(keys_wide, HEAD)
-            v = kv[pl.ds(2 * j, 2), 1].reshape(keys_wide, HEAD)
-            column_bias = bias[pl.ds(2 * j, 2)].reshape(keys_wide, HEAD)
-            s = nt(k, q) * (SCALE * LOG2E) - jnp.concatenate([column_bias] * (width // HEAD), axis=1)
-            if mask is not None:
-                s = jnp.where(mask, s, -1e30)
-            top = jnp.maximum(m, jnp.max(s, axis=0, keepdims=True))
-            w = jnp.exp2(s - top)
-            old = jnp.exp2(m - top)
-            dp = nt(v, g)
-            wbuf[slot, j] = w
-            dpbuf[slot, j] = dp
-            mrow[slot, j] = jnp.broadcast_to(top, (8, width))
-            total = total * old + jnp.sum(w, axis=0, keepdims=True)
-            terms = terms * old + jnp.sum(w * dp, axis=0, keepdims=True)
-            return top, total, terms
-
-        zero = jnp.zeros((1, width), jnp.float32)
-        state = lax.fori_loop(
-            0, t, lambda j, state: block(j, state, None), (jnp.full((1, width), -1e30, jnp.float32), zero, zero)
-        )
-        rows = halves * hk
-        key_row = lax.broadcasted_iota(jnp.int32, (keys_wide, width), 0)
-        query_row = lax.broadcasted_iota(jnp.int32, (keys_wide, width), 1)
-        key_pos = jnp.where(key_row >= hk, key_row - hk + rows, key_row) + half * hk
-        query_pos = jnp.where(query_row >= sub, query_row - sub + rows, query_row) + x * sub
-        m, total, terms = block(t, state, key_pos <= query_pos)
-        stat[t] = jnp.concatenate([m, total, terms, jnp.zeros((5, width), jnp.float32)], axis=0)
+        scores(j, j, True)
+
+        @pl.loop(j + 1, tiles)
+        def _(t):
+            scores(t, j, False)
+
+        @pl.when(j < tiles - 1)
+        def _():
+            stat_copy(j).start()
+
+        @pl.when(j < 2)
+        def _():
+            second_on(j + 2)
+
+        return carry
 
     def backward(t):
-        slot = lax.rem(t, 2)
-        q = qg[pl.ds(2 * t, 2), 0].reshape(width, HEAD)
-        g = qg[pl.ds(2 * t, 2), 1].reshape(width, HEAD)
+        q, g = queries(0, t), queries(1, t)
         arrived(stat_got.at[t], stat_recv.at[t])
         mine = stat[t]
         other = stat_got[t]
@@ -300,9 +318,9 @@
         terms = (mine[2:3] * scale_mine + other[2:3] * scale_other) * inverse
 
         def block(j, acc):
-            factor = jnp.exp2(mrow[slot, j][0:1] - top) * inverse
-            prob = wbuf[slot, j] * factor
-            ds = (prob * (dpbuf[slot, j] - terms)).astype(LOW)
+            factor = jnp.exp2(mrow[place(t, j)][0:1] - top) * inverse
+            prob = wbuf[place(t, j)] * factor
+            ds = (prob * (nt(pair(1, j), g) - terms)).astype(LOW)
             dv[j] += nn(prob.astype(LOW), g)
             dk[j] += nn(ds, q)
             return acc + nn(kt[j], ds)
@@ -423,37 +441,36 @@
             x_all.at[lax.rem(column + 2 * r, wide)], lax.rem(column + 2 * r, wide), twin, xf_send.at[r]
         )
 
+    lax.fori_loop(0, tiles, forward, 0)
+
+    for r in range(1, wide // 2):
+        source = lax.rem(column + 2 * r, wide)
+        pltpu.make_async_remote_copy(
+            src_ref=x_all.at[source], dst_ref=x_all.at[source], send_sem=xf_send.at[r],
+            recv_sem=x_recv.at[source], device_id={"tp": twin},
+        ).wait_recv()
+        x_on(r).start()
+    stat_copy(tiles - 1).start()
+
     def step(s, carry):
         t = tiles - 1 - s
 
         def stage(offset, work):
             pl.when((t + offset >= 0) & (t + offset < tiles))(lambda: work(t + offset))
 
-        stage(0, forward)
-        stage(2, dq_sends)
+        stage(1, dq_sends)
         stage(3, second_sends)
         stage(5, fin_sends)
-        stage(0, lambda tile: stat_copy(tile).start())
-        stage(1, backward)
-        stage(1, first_sends)
+        stage(0, backward)
+        stage(0, first_sends)
         stage(2, add_on_way)
         stage(4, reduce)
-
-        @pl.when(s == 2)
-        def _():
-            for r in range(1, wide // 2):
-                source = lax.rem(column + 2 * r, wide)
-                pltpu.make_async_remote_copy(
-                    src_ref=x_all.at[source], dst_ref=x_all.at[source], send_sem=xf_send.at[r],
-                    recv_sem=x_recv.at[source], device_id={"tp": twin},
-                ).wait_recv()
-                x_on(r).start()
-
         return carry
 
-    lax.fori_loop(0, tiles + 2, step, 0)
-    second_sends(0)
-    fin_sends(2)
+    lax.fori_loop(0, tiles + 1, step, 0)
+    second_sends(1)
+    fin_sends(3)
+    add_on_way(0)
 
     for r in range(nz):
         for c in range(nx):
@@ -467,7 +484,8 @@
                 value = value + dq_got[h * halves + m, n].astype(jnp.float32)
             low[n * sub : (n + 1) * sub, h * HEAD : (h + 1) * HEAD] = value.astype(LOW)
     low_copy = pltpu.make_async_copy(low, low_out, out_sem.at[0])
-    reduce(1)
+    second_sends(0)
+    reduce(2)
     for r in range(wide // 2):
         source = lax.rem(twin + 2 * r, wide)
         pltpu.make_async_remote_copy(
@@ -511,8 +529,8 @@
         waiting.extend(fresh)
     flush()
     low_copy.start()
-    fin_sends(1)
-    reduce(0)
+    fin_sends(2)
+    reduce(1)
 
     for n in list(range(1, nz)) + [0]:
         zt = near(n, 0)[0]
@@ -542,6 +560,8 @@
         waiting.extend(fresh)
     flush()
 
+    fin_sends(1)
+    reduce(0)
     fin_sends(0)
     for r in range(1, nz):
         zs = near(r, 0)[0]
@@ -564,6 +584,13 @@
         copy.wait_send()
     for r in range(1, wide // 2):
         x_on(r).wait_send()
+
+    @pl.loop(0, nz)
+    def _(p):
+        for i in range(2):
+            for c in (1, nx - 1):
+                round_copy(p, c, i).wait_send()
+            onward_copy(p, i).wait_send()
 
     @pl.loop(0, tiles)
     def _(t):
@@ -630,9 +657,8 @@
             pltpu.VMEM((blocks, 8, HEAD), f32),
             pltpu.VMEM((tiles, HEAD, 2 * hk), LOW),
             pltpu.VMEM((blocks, hk, HEAD), f32),
-            pltpu.VMEM((2, tiles, 2 * hk, 2 * sub), f32),
-            pltpu.VMEM((2, tiles, 2 * hk, 2 * sub), f32),
-            pltpu.VMEM((2, tiles, 8, 2 * sub), f32),
+            pltpu.VMEM((tiles * (tiles + 1) // 2, 2 * hk, 2 * sub), f32),
+            pltpu.VMEM((tiles * (tiles + 1) // 2, 8, 2 * sub), f32),
             pltpu.VMEM((tiles, 2 * hk, HEAD), f32),
             pltpu.VMEM((tiles, 2 * hk, HEAD), f32),
             pltpu.VMEM((tiles, 8, 2 * sub), f32),

time: 107 us -> 110 us (1.028)
  Pallas kernels: 106 us -> 109 us
    pallas_call x1, Pallas kernels: 104 us -> 107 us  [attention(): pl.pallas_call(lambda *refs: kernel_body(heads, wide, *refs), out_shape=(...]
where the time goes in v4:
time: 110 us
  Pallas kernels  109 us (99%)
    pallas_call x1, Pallas kernels, attention(): pl.pallas_call(lambda *refs: kernel_body(heads, wide, *refs), out_shape=(...  107 us
    pallas_call x1, Pallas kernels, finish(): pl.pallas_call(lambda *refs: finish_body(heads, *refs), out_shape=(grad,...  2.27 us

profile of v4, /device:TPU:0, one launch (start us, length us, event | category | flops | bytes accessed | tf_op | source)
XLA Modules:
  0.0 109.5 jit_solution(11039158671736993795)
XLA Ops:
  0.6 106.6 %attention.1 = (bf16[512,256]{1,0:T(8,128)(2,1)}, bf16[4,2,256,128]{3,2,1,0:T(8,128)(2,1)}, f32[256,256]{1,0:T(8,128)}) custom-call(bf16[512,256]{1,0:T(8,128)(2,1)} %refs_0_.1, bf16[512,256]{1,0:T(8,128)(2,1)} %refs_1_.1, bf16[512,256]{1,0:T(8,128)(2,1)} %refs_2_.1, bf16[512,256]{1,0:T(8,128)(2,1)} %refs_3_.1, f32[2,512]{1,0:T(2,128)} %bitcast.1, ...), custom_call_target="tpu_custom_call" | custom-call | flops 21474836480 | bytes 4194304 | tf_op jit(solution)/shard_map/attention/pallas_call | solution.py:638
  107.2 2.3 %finish.1 = (f32[512,256]{1,0:T(8,128)}, f32[512,256]{1,0:T(8,128)}, f32[512,256]{1,0:T(8,128)}, f32[256,256]{1,0:T(8,128)}) custom-call(bf16[512,256]{1,0:T(8,128)(2,1)} %get-tuple-element.7.refs_0_, bf16[4,2,256,128]{3,2,1,0:T(8,128)(2,1)} %get-tuple-element.8.refs_1_, f32[256,256]{1,0:T(8,128)} %get-tuple-element.9.refs_2_), custom_call_target="tpu_custom_call" | custom-call | tf_op jit(solution)/shard_map/finish/pallas_call | solution.py:738

commit v5 on v4

--- a/solution.py
+++ b/solution.py
@@ -24,7 +24,7 @@
     heads, wide,
     q_hbm, g_hbm, k_hbm, v_hbm, logits_hbm, x_hbm,
     low_out, kv_out, w_out,
-    q_in, g_in, k_in, v_in, logits, gate_in, w_sum, kv, qg, gates, kt, bias, wbuf, mrow, dk, dv, stat, stat_got,
+    q_in, g_in, k_in, v_in, logits, gate_in, w_sum, kv, qg, gates, kt, bias, wbuf, mrow, grads, stat, stat_got,
     dq_stage, part_stage, mid, red, fin, dq_got, kv_got,
     x_all, low, wa_stage, wb_stage, wa_red, wb_red, wa_own, wb_own, wa_fin, wb_fin, wa_got, wb_got,
     in_sem, out_sem, kv_recv, xs_send, col_send, x2_send, qg_recv, q_send, qf_send, gate_send, gate_recv, local_sem,
@@ -102,8 +102,8 @@
 
     @pl.loop(0, tiles)
     def _(j):
-        dk[j] = jnp.zeros((keys_wide, HEAD), jnp.float32)
-        dv[j] = jnp.zeros((keys_wide, HEAD), jnp.float32)
+        grads[0, j] = jnp.zeros((keys_wide, HEAD), jnp.float32)
+        grads[1, j] = jnp.zeros((keys_wide, HEAD), jnp.float32)
         stat[j] = jnp.where(line == 0, -1e30, 0.0)
 
     loads[0].wait()
@@ -142,6 +142,17 @@
             zt, xt = near(r, c)
             go(remote(gate_in.at[zt // halves], gates.at[me], gate_send.at[r, c], gate_recv.at[me], at(zt, xt)))
 
+    def kv_arrived(j, i):
+        arrived(kv.at[j, i], kv_recv.at[j, i])
+
+    def round_copy(p, c, i):
+        j = at(p, x)
+        return remote(kv.at[j, i], kv.at[j, i], xs_send.at[p, c // 2, i], kv_recv.at[j, i], at(z, near(0, c)[1]))
+
+    for i in range(2):
+        for c in (1, nx - 1):
+            round_copy(z, c, i).start()
+
     for r in (1, nz - 1, 2):
         zt = near(r, 0)[0]
         for i in range(2):
@@ -174,25 +185,15 @@
         go(x_copy(x_all.at[column], column, lax.rem(column + 2 * r, wide), x_send.at[r]))
     go(x_copy(x_all.at[column], column, twin, x_send.at[0]))
 
-    def kv_arrived(j, i):
-        arrived(kv.at[j, i], kv_recv.at[j, i])
-
-    def round_copy(p, c, i):
-        j = at(p, x)
-        return remote(kv.at[j, i], kv.at[j, i], xs_send.at[p, c // 2, i], kv_recv.at[j, i], at(z, near(0, c)[1]))
-
     def onward_copy(p, i):
         c = nx - 1 if i == 0 else 1
         j = at(p, near(0, c)[1])
         return remote(kv.at[j, i], kv.at[j, i], x2_send.at[p, i], kv_recv.at[j, i], at(z, near(0, nx - c)[1]))
 
-    def column_on(p):
-        @pl.when(z != p)
-        def _():
-            for i in range(2):
-                kv_arrived(at(p, x), i)
-
+    def column_on(r):
+        p = near(r, 0)[0]
         for i in range(2):
+            kv_arrived(at(p, x), i)
             for c in (1, nx - 1):
                 round_copy(p, c, i).start()
 
@@ -211,16 +212,16 @@
         for i in range(2):
             go(remote(qg.at[j, i], qg.at[j, i], qf_send.at[r, c, i], qg_recv.at[j, i], at(partner, x)))
 
-    column_on(0)
     column_on(1)
+    column_on(nz - 1)
     for c in range(1, nx):
+        if c == 2:
+            column_on(2)
         q_on(0, c)
     second_on(0)
-    column_on(2)
-    column_on(3)
+    second_on(1)
     for c in range(nx):
         q_on(1, c)
-    second_on(1)
     for r in range(nz):
         for c in range(nx):
             if (r, c) != (0, 0):
@@ -239,9 +240,8 @@
         return base + table[halves * per : halves * per + 1]
 
     lax.fori_loop(0, blocks, prepare, jnp.zeros((1, HEAD), jnp.float32))
-    for plane in (partner, nz - 1 - partner):
-        for c in range(nx):
-            q_wait(at(plane, near(0, c)[1]))
+    second_on(2)
+    second_on(3)
 
     rows = halves * hk
     key_row = lax.broadcasted_iota(jnp.int32, (keys_wide, width), 0)
@@ -258,13 +258,12 @@
     def place(t, j):
         return t * (t + 1) // 2 + j
 
-    def scores(t, j, masked):
+    def scores(t, j):
         state = stat[t]
         m, total, terms = state[0:1], state[1:2], state[2:3]
         column_bias = bias[pl.ds(2 * j, 2)].reshape(keys_wide, HEAD)
         s = nt(pair(0, j), queries(0, t)) * (SCALE * LOG2E) - jnp.concatenate([column_bias] * (width // HEAD), axis=1)
-        if masked:
-            s = jnp.where(key_pos <= query_pos, s, -1e30)
+        s = jnp.where(key_pos <= query_pos + (t - j) * (2 * rows), s, -1e30)
         top = jnp.maximum(m, jnp.max(s, axis=0, keepdims=True))
         w = jnp.exp2(s - top)
         old = jnp.exp2(m - top)
@@ -275,7 +274,7 @@
         terms = terms * old + jnp.sum(w * dp, axis=0, keepdims=True)
         stat[t] = jnp.concatenate([top, total, terms, jnp.zeros((5, width), jnp.float32)], axis=0)
 
-    def forward(j, carry):
+    def pair_wait(j):
         for u in range(2):
             b = 2 * j + u
             d = lax.rem(lax.rem(b, nx) + nx - x, nx)
@@ -290,21 +289,20 @@
 
         for n in range(2):
             kt[j, :, n * hk : (n + 1) * hk] = kv[2 * j + n, 0].T
-        scores(j, j, True)
-
-        @pl.loop(j + 1, tiles)
-        def _(t):
-            scores(t, j, False)
-
-        @pl.when(j < tiles - 1)
-        def _():
-            stat_copy(j).start()
-
-        @pl.when(j < 2)
-        def _():
-            second_on(j + 2)
-
-        return carry
+
+    outer = (z == 0) | (z == nz - 1)
+    quarter = tiles // 4
+
+    def group(direct, j):
+        ends = outer if direct else jnp.logical_not(outer)
+
+        @pl.loop(0, 2 * quarter)
+        def _(m):
+            t = jnp.where(ends, jnp.where(m >= quarter, m + 2 * quarter, m), m + quarter)
+
+            @pl.when(t >= j)
+            def _():
+                scores(t, j)
 
     def backward(t):
         q, g = queries(0, t), queries(1, t)
@@ -321,14 +319,14 @@
             factor = jnp.exp2(mrow[place(t, j)][0:1] - top) * inverse
             prob = wbuf[place(t, j)] * factor
             ds = (prob * (nt(pair(1, j), g) - terms)).astype(LOW)
-            dv[j] += nn(prob.astype(LOW), g)
-            dk[j] += nn(ds, q)
+            grads[1, j] += nn(prob.astype(LOW), g)
+            grads[0, j] += nn(ds, q)
             return acc + nn(kt[j], ds)
 
         acc = block(t, jnp.zeros((HEAD, width), jnp.float32))
-        for n in range(2):
-            part_stage[2 * t + n, 0] = (dk[t, n * hk : (n + 1) * hk] * SCALE).astype(LOW)
-            part_stage[2 * t + n, 1] = dv[t, n * hk : (n + 1) * hk].astype(LOW)
+        for n, (u, i) in enumerate(((0, 0), (1, 0), (1, 1), (0, 1))):
+            value = grads[i, t, u * hk : (u + 1) * hk]
+            part_stage[t, n] = (value * SCALE if i == 0 else value).astype(LOW)
         acc = lax.fori_loop(0, t, block, acc)
         dq_t = (acc * SCALE).T.astype(LOW)
         for n in range(2):
@@ -340,86 +338,83 @@
     def dq_copy(n):
         return remote(dq_stage.at[n], dq_got.at[z, x], dq_send.at[n], dq_recv.at[me], n)
 
-    def away(n):
-        return lax.rem(lax.rem(n, nx) + nx - x, nx)
-
-    def opposite_copy(n, i):
-        xt = lax.rem(x + (1 if i == 0 else nx - 1), nx)
-        return remote(part_stage.at[n, i], mid.at[n // nx, i], part_send.at[n, i], mid_recv.at[n // nx, i], at(z, xt))
-
-    def near_copy(n, side, i):
+    hr = hk // 2
+
+    def role(tile):
+        return lax.rem(x + nx - 2 * lax.rem(tile, nx // 2), nx)
+
+    def array(tile, c):
+        return lax.rem(role(tile) + c, nx)
+
+    def share(tile, n, way):
+        u = jnp.where((n == 1) | (n == 2), 1, 0)
+        i = n // 2
+        value = grads[i, tile, pl.ds(pl.multiple_of(u * hk + way * hr, hr), hr)]
+        return value * jnp.where(i == 0, SCALE, 1.0)
+
+    def half_of(tile, n, way):
+        return part_stage.at[tile, n, pl.ds(way * hr, hr)]
+
+    def opposite_copy(tile, way):
+        n = array(tile, 2)
         return remote(
-            part_stage.at[n, i], red.at[n // nx, side, i], part_send.at[n, i], red_recv.at[n // nx, side, i],
-            at(z, lax.rem(n, nx)),
+            half_of(tile, n, way), mid.at[tile, way], part_send.at[tile, n, way], mid_recv.at[tile, way],
+            at(z, near(0, nx - 1 if way else 1)[1]),
         )
 
+    def near_copy(tile, side, way):
+        c = nx - 1 if side else 1
+        n = array(tile, c)
+        return remote(
+            half_of(tile, n, way), red.at[tile, side, way], part_send.at[tile, n, way], red_recv.at[tile, side, way],
+            at(z, near(0, c)[1]),
+        )
+
     def first_sends(tile):
-        for u in range(2):
-            n = 2 * tile + u
-
-            @pl.when(away(n) == 2)
-            def _():
-                opposite_copy(n, 0).start()
-                opposite_copy(n, 1).start()
-
-            @pl.when(away(n) == 1)
-            def _():
-                near_copy(n, 0, 1).start()
-
-            @pl.when(away(n) == nx - 1)
-            def _():
-                near_copy(n, 1, 0).start()
+        for way in range(2):
+            opposite_copy(tile, way).start()
+        near_copy(tile, 0, 1).start()
+        near_copy(tile, 1, 0).start()
 
     def add_on_way(tile):
-        for u in range(2):
-            n = 2 * tile + u
-            zn = n // nx
-            for i, d in ((0, 1), (1, nx - 1)):
-
-                @pl.when(away(n) == d)
-                def _():
-                    arrived(mid.at[zn, i], mid_recv.at[zn, i])
-                    value = dk[tile, u * hk : (u + 1) * hk] * SCALE if i == 0 else dv[tile, u * hk : (u + 1) * hk]
-                    part_stage[n, i] = (value + mid[zn, i].astype(jnp.float32)).astype(LOW)
+        for way, c in ((0, 1), (1, nx - 1)):
+            n = array(tile, c)
+            arrived(mid.at[tile, way], mid_recv.at[tile, way])
+            part_stage[tile, n, way * hr : (way + 1) * hr] = (
+                share(tile, n, way) + mid[tile, way].astype(jnp.float32)
+            ).astype(LOW)
 
     def second_sends(tile):
-        for u in range(2):
-            n = 2 * tile + u
-
-            @pl.when(away(n) == 1)
-            def _():
-                near_copy(n, 0, 0).start()
-
-            @pl.when(away(n) == nx - 1)
-            def _():
-                near_copy(n, 1, 1).start()
+        near_copy(tile, 0, 0).start()
+        near_copy(tile, 1, 1).start()
 
     def reduce(tile):
-        for u in range(2):
-            n = 2 * tile + u
-
-            @pl.when(away(n) == 0)
-            def _():
-                zn = n // nx
-                for i in range(2):
-                    for side in range(2):
-                        arrived(red.at[zn, side, i], red_recv.at[zn, side, i])
-                    value = dk[tile, u * hk : (u + 1) * hk] * SCALE if i == 0 else dv[tile, u * hk : (u + 1) * hk]
-                    for side in range(2):
-                        value = value + red[zn, side, i].astype(jnp.float32)
-                    fin[zn, i] = value.astype(LOW)
+        n = array(tile, 0)
+        for way in range(2):
+            value = share(tile, n, way)
+            for side in range(2):
+                arrived(red.at[tile, side, way], red_recv.at[tile, side, way])
+                value = value + red[tile, side, way].astype(jnp.float32)
+            fin[tile, way * hr : (way + 1) * hr] = value.astype(LOW)
+
+    def fin_owner(tile):
+        n = array(tile, 0)
+        return 2 * tile + jnp.where((n == 1) | (n == 2), 1, 0), n // 2
+
+    def fin_copy(tile):
+        owner, i = fin_owner(tile)
+        return remote(fin.at[tile], kv_got.at[z, i], fin_send.at[tile], fin_recv.at[z, i], owner)
 
     def fin_sends(tile):
-        for u in range(2):
-            n = 2 * tile + u
-
-            @pl.when((away(n) == 0) & (n == me))
-            def _():
-                kv_got[z] = fin[n // nx]
-
-            @pl.when((away(n) == 0) & (n != me))
-            def _():
-                fin_copy(n).start()
+        owner, i = fin_owner(tile)
+
+        @pl.when(owner == me)
+        def _():
+            kv_got[z, i] = fin[tile]
+
+        @pl.when(owner != me)
+        def _():
+            fin_copy(tile).start()
 
     def dq_sends(tile):
         for u in range(2):
@@ -432,16 +427,38 @@
             @pl.when(n != me)
             def _():
                 dq_copy(n).start()
-
-    def fin_copy(n):
-        return remote(fin.at[n // nx], kv_got.at[z], fin_send.at[n // nx], fin_recv.at[z], n)
 
     def x_on(r):
         return x_copy(
             x_all.at[lax.rem(column + 2 * r, wide)], lax.rem(column + 2 * r, wide), twin, xf_send.at[r]
         )
 
-    lax.fori_loop(0, tiles, forward, 0)
+    @pl.loop(0, tiles // 2)
+    def _(j):
+        pair_wait(j)
+        group(True, j)
+
+    for plane in (partner, nz - 1 - partner):
+        for c in range(nx):
+            q_wait(at(plane, near(0, c)[1]))
+
+    @pl.loop(0, tiles // 2)
+    def _(j):
+        group(False, j)
+
+    @pl.loop(tiles // 2, tiles)
+    def _(j):
+        pair_wait(j)
+
+        @pl.loop(j, tiles)
+        def _(t):
+            scores(t, j)
+
+        stat_copy(j - tiles // 2).start()
+
+        @pl.when(j < tiles - 1)
+        def _():
+            stat_copy(j).start()
 
     for r in range(1, wide // 2):
         source = lax.rem(column + 2 * r, wide)
@@ -563,9 +580,18 @@
     fin_sends(1)
     reduce(0)
     fin_sends(0)
-    for r in range(1, nz):
+    my_tile = me // 2
+    for r in range(nz):
         zs = near(r, 0)[0]
-        arrived(kv_got.at[zs], fin_recv.at[zs])
+        for i in range(2):
+            if r == 0:
+                owner, mine = fin_owner(my_tile)
+
+                @pl.when(jnp.logical_not((owner == me) & (mine == i)))
+                def _():
+                    arrived(kv_got.at[zs, i], fin_recv.at[zs, i])
+            else:
+                arrived(kv_got.at[zs, i], fin_recv.at[zs, i])
     kv_copy = pltpu.make_async_copy(kv_got, kv_out, out_sem.at[1])
     kv_copy.start()
     for n in range(1, nz):
@@ -602,21 +628,16 @@
         def _():
             dq_copy(n).wait_send()
 
-        @pl.when(away(n) == 2)
+    @pl.loop(0, tiles)
+    def _(tile):
+        for way in range(2):
+            opposite_copy(tile, way).wait_send()
+            for side in range(2):
+                near_copy(tile, side, way).wait_send()
+
+        @pl.when(fin_owner(tile)[0] != me)
         def _():
-            for i in range(2):
-                opposite_copy(n, i).wait_send()
-
-        for d, side in ((1, 0), (nx - 1, 1)):
-
-            @pl.when(away(n) == d)
-            def _():
-                for i in range(2):
-                    near_copy(n, side, i).wait_send()
-
-        @pl.when((away(n) == 0) & (n != me))
-        def _():
-            fin_copy(n).wait_send()
+            fin_copy(tile).wait_send()
 
     w_copy.wait()
 
@@ -659,15 +680,14 @@
             pltpu.VMEM((blocks, hk, HEAD), f32),
             pltpu.VMEM((tiles * (tiles + 1) // 2, 2 * hk, 2 * sub), f32),
             pltpu.VMEM((tiles * (tiles + 1) // 2, 8, 2 * sub), f32),
-            pltpu.VMEM((tiles, 2 * hk, HEAD), f32),
-            pltpu.VMEM((tiles, 2 * hk, HEAD), f32),
+            pltpu.VMEM((2, tiles, 2 * hk, HEAD), f32),
             pltpu.VMEM((tiles, 8, 2 * sub), f32),
             pltpu.VMEM((tiles, 8, 2 * sub), f32),
             pltpu.VMEM((blocks, sub, HEAD), LOW),
-            pltpu.VMEM((blocks, 2, hk, HEAD), LOW),
-            pltpu.VMEM((nz, 2, hk, HEAD), LOW),
-            pltpu.VMEM((nz, 2, 2, hk, HEAD), LOW),
-            pltpu.VMEM((nz, 2, hk, HEAD), LOW),
+            pltpu.VMEM((tiles, nx, hk, HEAD), LOW),
+            pltpu.VMEM((tiles, 2, hk // 2, HEAD), LOW),
+            pltpu.VMEM((tiles, 2, 2, hk // 2, HEAD), LOW),
+            pltpu.VMEM((tiles, hk, HEAD), LOW),
             pltpu.VMEM((nz, nx, sub, HEAD), LOW),
             pltpu.VMEM((nz, 2, hk, HEAD), LOW),
             pltpu.VMEM((wide, rows, x.shape[1]), LOW),
@@ -685,8 +705,8 @@
             dma((6,)), dma((3,)),
             dma((blocks, 2)), dma((nz, 2, 2)), dma((nz, 2)), dma((nz, 2)), dma((blocks, 2)), dma((heads, nx, 2)),
             dma((heads, nx, 2)), dma((nz, nx)), dma((blocks,)), dma((6,)),
-            dma((tiles,)), dma((tiles,)), dma((blocks,)), dma((blocks,)), dma((blocks, 2)), dma((nz, 2)), dma((nz, 2, 2)),
-            dma((nz,)), dma((nz,)),
+            dma((tiles,)), dma((tiles,)), dma((blocks,)), dma((blocks,)), dma((tiles, nx, 2)), dma((tiles, 2)),
+            dma((tiles, 2, 2)), dma((tiles,)), dma((nz, 2)),
             dma((wide // 2,)), dma((wide // 2,)), dma((wide,)),
             dma((nz, nx)), dma((nz, nx)), dma((nx, nz)), dma((nz, nx)),
             dma((nz,)), dma((nx,)), dma((nz,)), dma((nx,)),

time: 110 us -> 111 us (level)
    pallas_call x1, Pallas kernels: 107 us -> 108 us  [attention(): pl.pallas_call(lambda *refs: kernel_body(heads, wide, *refs), out_shape=(...]
where the time goes in v5:
time: 111 us
  Pallas kernels  110 us (99%)
    pallas_call x1, Pallas kernels, attention(): pl.pallas_call(lambda *refs: kernel_body(heads, wide, *refs), out_shape=(...  108 us
    pallas_call x1, Pallas kernels, finish(): pl.pallas_call(lambda *refs: finish_body(heads, *refs), out_shape=(grad,...  2.27 us

profile of v5, /device:TPU:0, one launch (start us, length us, event | category | flops | bytes accessed | tf_op | source)
XLA Modules:
  0.0 110.9 jit_solution(7785225331767830048)
XLA Ops:
  0.6 108.0 %attention.1 = (bf16[512,256]{1,0:T(8,128)(2,1)}, bf16[4,2,256,128]{3,2,1,0:T(8,128)(2,1)}, f32[256,256]{1,0:T(8,128)}) custom-call(bf16[512,256]{1,0:T(8,128)(2,1)} %refs_0_.1, bf16[512,256]{1,0:T(8,128)(2,1)} %refs_1_.1, bf16[512,256]{1,0:T(8,128)(2,1)} %refs_2_.1, bf16[512,256]{1,0:T(8,128)(2,1)} %refs_3_.1, f32[2,512]{1,0:T(2,128)} %bitcast.1, ...), custom_call_target="tpu_custom_call" | custom-call | flops 21474836480 | bytes 4194304 | tf_op jit(solution)/shard_map/attention/pallas_call | solution.py:659
  108.7 2.3 %finish.1 = (f32[512,256]{1,0:T(8,128)}, f32[512,256]{1,0:T(8,128)}, f32[512,256]{1,0:T(8,128)}, f32[256,256]{1,0:T(8,128)}) custom-call(bf16[512,256]{1,0:T(8,128)(2,1)} %get-tuple-element.7.refs_0_, bf16[4,2,256,128]{3,2,1,0:T(8,128)(2,1)} %get-tuple-element.8.refs_1_, f32[256,256]{1,0:T(8,128)} %get-tuple-element.9.refs_2_), custom_call_target="tpu_custom_call" | custom-call | tf_op jit(solution)/shard_map/finish/pallas_call | solution.py:758

commit v6 on v5

--- a/solution.py
+++ b/solution.py
@@ -240,9 +240,6 @@
         return base + table[halves * per : halves * per + 1]
 
     lax.fori_loop(0, blocks, prepare, jnp.zeros((1, HEAD), jnp.float32))
-    second_on(2)
-    second_on(3)
-
     rows = halves * hk
     key_row = lax.broadcasted_iota(jnp.int32, (keys_wide, width), 0)
     query_row = lax.broadcasted_iota(jnp.int32, (keys_wide, width), 1)
@@ -438,6 +435,10 @@
         pair_wait(j)
         group(True, j)
 
+        @pl.when(lax.rem(j, 2) == 1)
+        def _():
+            second_on(2 + j // 2)
+
     for plane in (partner, nz - 1 - partner):
         for c in range(nx):
             q_wait(at(plane, near(0, c)[1]))
@@ -476,17 +477,15 @@
             pl.when((t + offset >= 0) & (t + offset < tiles))(lambda: work(t + offset))
 
         stage(1, dq_sends)
-        stage(3, second_sends)
-        stage(5, fin_sends)
+        stage(4, second_sends)
         stage(0, backward)
         stage(0, first_sends)
-        stage(2, add_on_way)
-        stage(4, reduce)
+        stage(3, add_on_way)
         return carry
 
     lax.fori_loop(0, tiles + 1, step, 0)
-    second_sends(1)
-    fin_sends(3)
+    second_sends(2)
+    add_on_way(1)
     add_on_way(0)
 
     for r in range(nz):
@@ -501,8 +500,8 @@
                 value = value + dq_got[h * halves + m, n].astype(jnp.float32)
             low[n * sub : (n + 1) * sub, h * HEAD : (h + 1) * HEAD] = value.astype(LOW)
     low_copy = pltpu.make_async_copy(low, low_out, out_sem.at[0])
+    second_sends(1)
     second_sends(0)
-    reduce(2)
     for r in range(wide // 2):
         source = lax.rem(twin + 2 * r, wide)
         pltpu.make_async_remote_copy(
@@ -546,10 +545,19 @@
         waiting.extend(fresh)
     flush()
     low_copy.start()
-    fin_sends(2)
-    reduce(1)
+
+    @pl.loop(0, tiles)
+    def _(n):
+        reduce(tiles - 1 - n)
+
+        @pl.when(n > 0)
+        def _():
+            fin_sends(tiles - n)
+
 
     for n in list(range(1, nz)) + [0]:
+        if n == 2:
+            fin_sends(0)
         zt = near(n, 0)[0]
         value = wa_own[n]
         for c in range(1, nx):
@@ -577,9 +585,6 @@
         waiting.extend(fresh)
     flush()
 
-    fin_sends(1)
-    reduce(0)
-    fin_sends(0)
     my_tile = me // 2
     for r in range(nz):
         zs = near(r, 0)[0]

time: 111 us -> 108 us (0.973)
  Pallas kernels: 110 us -> 107 us
    pallas_call x1, Pallas kernels: 108 us -> 105 us  [attention(): pl.pallas_call(lambda *refs: kernel_body(heads, wide, *refs), out_shape=(...]
where the time goes in v6:
time: 108 us
  Pallas kernels  107 us (99%)
    pallas_call x1, Pallas kernels, attention(): pl.pallas_call(lambda *refs: kernel_body(heads, wide, *refs), out_shape=(...  105 us
    pallas_call x1, Pallas kernels, finish(): pl.pallas_call(lambda *refs: finish_body(heads, *refs), out_shape=(grad,...  2.27 us

profile of v6, /device:TPU:0, one launch (start us, length us, event | category | flops | bytes accessed | tf_op | source)
XLA Modules:
  0.0 107.9 jit_solution(260186046387068816)
XLA Ops:
  0.6 105.0 %attention.1 = (bf16[512,256]{1,0:T(8,128)(2,1)}, bf16[4,2,256,128]{3,2,1,0:T(8,128)(2,1)}, f32[256,256]{1,0:T(8,128)}) custom-call(bf16[512,256]{1,0:T(8,128)(2,1)} %refs_0_.1, bf16[512,256]{1,0:T(8,128)(2,1)} %refs_1_.1, bf16[512,256]{1,0:T(8,128)(2,1)} %refs_2_.1, bf16[512,256]{1,0:T(8,128)(2,1)} %refs_3_.1, f32[2,512]{1,0:T(2,128)} %bitcast.1, ...), custom_call_target="tpu_custom_call" | custom-call | flops 21474836480 | bytes 4194304 | tf_op jit(solution)/shard_map/attention/pallas_call | solution.py:664
  105.7 2.3 %finish.1 = (f32[512,256]{1,0:T(8,128)}, f32[512,256]{1,0:T(8,128)}, f32[512,256]{1,0:T(8,128)}, f32[256,256]{1,0:T(8,128)}) custom-call(bf16[512,256]{1,0:T(8,128)(2,1)} %get-tuple-element.7.refs_0_, bf16[4,2,256,128]{3,2,1,0:T(8,128)(2,1)} %get-tuple-element.8.refs_1_, f32[256,256]{1,0:T(8,128)} %get-tuple-element.9.refs_2_), custom_call_target="tpu_custom_call" | custom-call | tf_op jit(solution)/shard_map/finish/pallas_call | solution.py:763

commit v7 on v6

--- a/solution.py
+++ b/solution.py
@@ -24,7 +24,7 @@
     heads, wide,
     q_hbm, g_hbm, k_hbm, v_hbm, logits_hbm, x_hbm,
     low_out, kv_out, w_out,
-    q_in, g_in, k_in, v_in, logits, gate_in, w_sum, kv, qg, gates, kt, bias, wbuf, mrow, grads, stat, stat_got,
+    q_in, g_in, k_in, v_in, logits, gate_in, w_sum, kv, qg, gates, kt, bias, wbuf, mrow, grads, acc, stat, stat_got,
     dq_stage, part_stage, mid, red, fin, dq_got, kv_got,
     x_all, low, wa_stage, wb_stage, wa_red, wb_red, wa_own, wb_own, wa_fin, wb_fin, wa_got, wb_got,
     in_sem, out_sem, kv_recv, xs_send, col_send, x2_send, qg_recv, q_send, qf_send, gate_send, gate_recv, local_sem,
@@ -218,10 +218,6 @@
         if c == 2:
             column_on(2)
         q_on(0, c)
-    second_on(0)
-    second_on(1)
-    for c in range(nx):
-        q_on(1, c)
     for r in range(nz):
         for c in range(nx):
             if (r, c) != (0, 0):
@@ -240,6 +236,10 @@
         return base + table[halves * per : halves * per + 1]
 
     lax.fori_loop(0, blocks, prepare, jnp.zeros((1, HEAD), jnp.float32))
+    second_on(0)
+    second_on(1)
+    for c in range(nx):
+        q_on(1, c)
     rows = halves * hk
     key_row = lax.broadcasted_iota(jnp.int32, (keys_wide, width), 0)
     query_row = lax.broadcasted_iota(jnp.int32, (keys_wide, width), 1)
@@ -255,21 +255,28 @@
     def place(t, j):
         return t * (t + 1) // 2 + j
 
-    def scores(t, j):
-        state = stat[t]
-        m, total, terms = state[0:1], state[1:2], state[2:3]
+    def scores(j, *group):
+        k, v = pair(0, j), pair(1, j)
         column_bias = bias[pl.ds(2 * j, 2)].reshape(keys_wide, HEAD)
-        s = nt(pair(0, j), queries(0, t)) * (SCALE * LOG2E) - jnp.concatenate([column_bias] * (width // HEAD), axis=1)
-        s = jnp.where(key_pos <= query_pos + (t - j) * (2 * rows), s, -1e30)
-        top = jnp.maximum(m, jnp.max(s, axis=0, keepdims=True))
-        w = jnp.exp2(s - top)
-        old = jnp.exp2(m - top)
-        dp = nt(pair(1, j), queries(1, t))
-        wbuf[place(t, j)] = w
-        mrow[place(t, j)] = jnp.broadcast_to(top, (8, width))
-        total = total * old + jnp.sum(w, axis=0, keepdims=True)
-        terms = terms * old + jnp.sum(w * dp, axis=0, keepdims=True)
-        stat[t] = jnp.concatenate([top, total, terms, jnp.zeros((5, width), jnp.float32)], axis=0)
+        column_bias = jnp.concatenate([column_bias] * (width // HEAD), axis=1)
+        states = [stat[t] for t, _ in group]
+        results = []
+        for (t, masked), state in zip(group, states):
+            m, total, terms = state[0:1], state[1:2], state[2:3]
+            s = nt(k, queries(0, t)) * (SCALE * LOG2E) - column_bias
+            if masked:
+                s = jnp.where(key_pos <= query_pos, s, -1e30)
+            top = jnp.maximum(m, jnp.max(s, axis=0, keepdims=True))
+            w = jnp.exp2(s - top)
+            old = jnp.exp2(m - top)
+            dp = nt(v, queries(1, t))
+            total = total * old + jnp.sum(w, axis=0, keepdims=True)
+            terms = terms * old + jnp.sum(w * dp, axis=0, keepdims=True)
+            wbuf[place(t, j)] = w
+            results.append((top, total, terms))
+        for (t, _), (top, total, terms) in zip(group, results):
+            mrow[place(t, j)] = jnp.broadcast_to(top, (8, width))
+            stat[t] = jnp.concatenate([top, total, terms, jnp.zeros((5, width), jnp.float32)], axis=0)
 
     def pair_wait(j):
         for u in range(2):
@@ -293,13 +300,21 @@
     def group(direct, j):
         ends = outer if direct else jnp.logical_not(outer)
 
-        @pl.loop(0, 2 * quarter)
+        @pl.loop(0, quarter)
         def _(m):
-            t = jnp.where(ends, jnp.where(m >= quarter, m + 2 * quarter, m), m + quarter)
-
-            @pl.when(t >= j)
+            t = jnp.where(ends, m * 3 * quarter, quarter + m * 2)
+
+            @pl.when(t > j)
             def _():
-                scores(t, j)
+                scores(j, (t, False), (t + 1, False))
+
+            @pl.when(t == j)
+            def _():
+                scores(j, (t, True), (t + 1, False))
+
+            @pl.when(t + 1 == j)
+            def _():
+                scores(j, (t + 1, True))
 
     def backward(t):
         q, g = queries(0, t), queries(1, t)
@@ -312,20 +327,33 @@
         inverse = 1.0 / (mine[1:2] * scale_mine + other[1:2] * scale_other)
         terms = (mine[2:3] * scale_mine + other[2:3] * scale_other) * inverse
 
-        def block(j, acc):
-            factor = jnp.exp2(mrow[place(t, j)][0:1] - top) * inverse
-            prob = wbuf[place(t, j)] * factor
-            ds = (prob * (nt(pair(1, j), g) - terms)).astype(LOW)
-            grads[1, j] += nn(prob.astype(LOW), g)
-            grads[0, j] += nn(ds, q)
-            return acc + nn(kt[j], ds)
-
-        acc = block(t, jnp.zeros((HEAD, width), jnp.float32))
+        def blocks_of(*pairs):
+            added = []
+            for j in pairs:
+                factor = jnp.exp2(mrow[place(t, j)][0:1] - top) * inverse
+                prob = wbuf[place(t, j)] * factor
+                ds = (prob * (nt(pair(1, j), g) - terms)).astype(LOW)
+                added.append((j, nn(prob.astype(LOW), g), nn(ds, q), nn(kt[j], ds)))
+            for j, dv, dk, _ in added:
+                grads[1, j] += dv
+                grads[0, j] += dk
+            acc[...] += sum(term for _, _, _, term in added)
+
+        acc[...] = jnp.zeros((HEAD, width), jnp.float32)
+        blocks_of(t)
         for n, (u, i) in enumerate(((0, 0), (1, 0), (1, 1), (0, 1))):
             value = grads[i, t, u * hk : (u + 1) * hk]
             part_stage[t, n] = (value * SCALE if i == 0 else value).astype(LOW)
-        acc = lax.fori_loop(0, t, block, acc)
-        dq_t = (acc * SCALE).T.astype(LOW)
+
+        @pl.loop(0, t // 2)
+        def _(n):
+            blocks_of(2 * n, 2 * n + 1)
+
+        @pl.when(lax.rem(t, 2) == 1)
+        def _():
+            blocks_of(t - 1)
+
+        dq_t = (acc[...] * SCALE).T.astype(LOW)
         for n in range(2):
             dq_stage[2 * t + n] = dq_t[n * sub : (n + 1) * sub]
 
@@ -451,9 +479,20 @@
     def _(j):
         pair_wait(j)
 
-        @pl.loop(j, tiles)
-        def _(t):
-            scores(t, j)
+        odd = lax.rem(tiles - 1 - j, 2)
+
+        @pl.when(odd == 1)
+        def _():
+            scores(j, (j, True), (j + 1, False))
+
+        @pl.when(odd == 0)
+        def _():
+            scores(j, (j, True))
+
+        @pl.loop(0, (tiles - 1 - j) // 2)
+        def _(n):
+            t = j + 1 + odd + 2 * n
+            scores(j, (t, False), (t + 1, False))
 
         stat_copy(j - tiles // 2).start()
 
@@ -476,17 +515,26 @@
         def stage(offset, work):
             pl.when((t + offset >= 0) & (t + offset < tiles))(lambda: work(t + offset))
 
-        stage(1, dq_sends)
         stage(4, second_sends)
+        stage(7, fin_sends)
         stage(0, backward)
         stage(0, first_sends)
+        stage(0, dq_sends)
         stage(3, add_on_way)
+        stage(6, reduce)
         return carry
 
-    lax.fori_loop(0, tiles + 1, step, 0)
+    lax.fori_loop(0, tiles, step, 0)
+    second_sends(3)
+    add_on_way(2)
+    add_on_way(1)
     second_sends(2)
-    add_on_way(1)
     add_on_way(0)
+    second_sends(1)
+    fin_sends(6)
+    second_sends(0)
+    reduce(5)
+    reduce(4)
 
     for r in range(nz):
         for c in range(nx):
@@ -500,8 +548,8 @@
                 value = value + dq_got[h * halves + m, n].astype(jnp.float32)
             low[n * sub : (n + 1) * sub, h * HEAD : (h + 1) * HEAD] = value.astype(LOW)
     low_copy = pltpu.make_async_copy(low, low_out, out_sem.at[0])
-    second_sends(1)
-    second_sends(0)
+    fin_sends(5)
+    fin_sends(4)
     for r in range(wide // 2):
         source = lax.rem(twin + 2 * r, wide)
         pltpu.make_async_remote_copy(
@@ -546,13 +594,13 @@
     flush()
     low_copy.start()
 
-    @pl.loop(0, tiles)
+    @pl.loop(0, 4)
     def _(n):
-        reduce(tiles - 1 - n)
+        reduce(3 - n)
 
         @pl.when(n > 0)
         def _():
-            fin_sends(tiles - n)
+            fin_sends(4 - n)
 
 
     for n in list(range(1, nz)) + [0]:
@@ -686,6 +734,7 @@
             pltpu.VMEM((tiles * (tiles + 1) // 2, 2 * hk, 2 * sub), f32),
             pltpu.VMEM((tiles * (tiles + 1) // 2, 8, 2 * sub), f32),
             pltpu.VMEM((2, tiles, 2 * hk, HEAD), f32),
+            pltpu.VMEM((HEAD, 2 * sub), f32),
             pltpu.VMEM((tiles, 8, 2 * sub), f32),
             pltpu.VMEM((tiles, 8, 2 * sub), f32),
             pltpu.VMEM((blocks, sub, HEAD), LOW),

time: 108 us -> 103 us (0.954)
  Pallas kernels: 107 us -> 103 us
    pallas_call x1, Pallas kernels: 105 us -> 100 us  [attention(): pl.pallas_call(lambda *refs: kernel_body(heads, wide, *refs), out_shape=(...]
where the time goes in v7:
time: 103 us
  Pallas kernels  103 us (100%)
    pallas_call x1, Pallas kernels, attention(): pl.pallas_call(lambda *refs: kernel_body(heads, wide, *refs), out_shape=(...  100 us
    pallas_call x1, Pallas kernels, finish(): pl.pallas_call(lambda *refs: finish_body(heads, *refs), out_shape=(grad,...  2.27 us

profile of v7, /device:TPU:0, one launch (start us, length us, event | category | flops | bytes accessed | tf_op | source)
XLA Modules:
  0.0 103.2 jit_solution(13125982007526411800)
XLA Ops:
  0.6 100.3 %attention.1 = (bf16[512,256]{1,0:T(8,128)(2,1)}, bf16[4,2,256,128]{3,2,1,0:T(8,128)(2,1)}, f32[256,256]{1,0:T(8,128)}) custom-call(bf16[512,256]{1,0:T(8,128)(2,1)} %refs_0_.1, bf16[512,256]{1,0:T(8,128)(2,1)} %refs_1_.1, bf16[512,256]{1,0:T(8,128)(2,1)} %refs_2_.1, bf16[512,256]{1,0:T(8,128)(2,1)} %refs_3_.1, f32[2,512]{1,0:T(2,128)} %bitcast.1, ...), custom_call_target="tpu_custom_call" | custom-call | flops 21474836480 | bytes 4194304 | tf_op jit(solution)/shard_map/attention/pallas_call | solution.py:712
  101.0 2.3 %finish.1 = (f32[512,256]{1,0:T(8,128)}, f32[512,256]{1,0:T(8,128)}, f32[512,256]{1,0:T(8,128)}, f32[256,256]{1,0:T(8,128)}) custom-call(bf16[512,256]{1,0:T(8,128)(2,1)} %get-tuple-element.7.refs_0_, bf16[4,2,256,128]{3,2,1,0:T(8,128)(2,1)} %get-tuple-element.8.refs_1_, f32[256,256]{1,0:T(8,128)} %get-tuple-element.9.refs_2_), custom_call_target="tpu_custom_call" | custom-call | tf_op jit(solution)/shard_map/finish/pallas_call | solution.py:812

commit v8 on v7

--- a/solution.py
+++ b/solution.py
@@ -316,6 +316,11 @@
             def _():
                 scores(j, (t + 1, True))
 
+    def stage_parts(t):
+        for n, (u, i) in enumerate(((0, 0), (1, 0), (1, 1), (0, 1))):
+            value = grads[i, t, u * hk : (u + 1) * hk]
+            part_stage[t, n] = (value * SCALE if i == 0 else value).astype(LOW)
+
     def backward(t):
         q, g = queries(0, t), queries(1, t)
         arrived(stat_got.at[t], stat_recv.at[t])
@@ -341,9 +346,10 @@
 
         acc[...] = jnp.zeros((HEAD, width), jnp.float32)
         blocks_of(t)
-        for n, (u, i) in enumerate(((0, 0), (1, 0), (1, 1), (0, 1))):
-            value = grads[i, t, u * hk : (u + 1) * hk]
-            part_stage[t, n] = (value * SCALE if i == 0 else value).astype(LOW)
+
+        @pl.when((t >= tiles // 2) | (t < tiles // 4))
+        def _():
+            stage_parts(t)
 
         @pl.loop(0, t // 2)
         def _(n):
@@ -509,32 +515,35 @@
         x_on(r).start()
     stat_copy(tiles - 1).start()
 
+    middle, low_tiles = tiles // 4, tiles // 4
+    upper = tiles // 2
+
     def step(s, carry):
-        t = tiles - 1 - s
-
-        def stage(offset, work):
-            pl.when((t + offset >= 0) & (t + offset < tiles))(lambda: work(t + offset))
+        last = middle + upper
+        t = jnp.where(
+            s < middle, upper - 1 - s, jnp.where(s < last, tiles - 1 + middle - s, last + low_tiles - 1 - s)
+        )
+        sent_tile = tiles - 1 + middle - s
+
+        def stage(lag, work, begin=upper):
+            tile = sent_tile + lag
+            pl.when((tile >= begin) & (tile < tiles))(lambda: work(tile))
 
         stage(4, second_sends)
-        stage(7, fin_sends)
-        stage(0, backward)
+        backward(t)
+        dq_sends(t)
         stage(0, first_sends)
-        stage(0, dq_sends)
         stage(3, add_on_way)
-        stage(6, reduce)
         return carry
 
     lax.fori_loop(0, tiles, step, 0)
-    second_sends(3)
-    add_on_way(2)
-    add_on_way(1)
-    second_sends(2)
-    add_on_way(0)
-    second_sends(1)
-    fin_sends(6)
-    second_sends(0)
-    reduce(5)
-    reduce(4)
+    for tile in range(upper - 1, low_tiles - 1, -1):
+        stage_parts(tile)
+    second_sends(5)
+    for tile in range(low_tiles - 1, -1, -1):
+        first_sends(tile)
+    for tile in range(upper - 1, low_tiles - 1, -1):
+        first_sends(tile)
 
     for r in range(nz):
         for c in range(nx):
@@ -548,8 +557,6 @@
                 value = value + dq_got[h * halves + m, n].astype(jnp.float32)
             low[n * sub : (n + 1) * sub, h * HEAD : (h + 1) * HEAD] = value.astype(LOW)
     low_copy = pltpu.make_async_copy(low, low_out, out_sem.at[0])
-    fin_sends(5)
-    fin_sends(4)
     for r in range(wide // 2):
         source = lax.rem(twin + 2 * r, wide)
         pltpu.make_async_remote_copy(
@@ -569,9 +576,20 @@
             go(copy)
         waiting.clear()
 
+    between = {
+        1: (lambda: add_on_way(4), lambda: reduce(7)),
+        3: (lambda: second_sends(4), lambda: fin_sends(7), lambda: add_on_way(1)),
+        5: (lambda: second_sends(1), lambda: reduce(6), lambda: add_on_way(0)),
+        7: (lambda: second_sends(0), lambda: fin_sends(6), lambda: add_on_way(3)),
+        9: (lambda: second_sends(3), lambda: reduce(5), lambda: add_on_way(2)),
+        11: (lambda: second_sends(2), lambda: fin_sends(5), lambda: reduce(4)),
+        13: (lambda: fin_sends(4),),
+    }
     order = [(r, c) for r in range(1, nz) for c in range(1, nx)]
     order += [(0, c) for c in range(1, nx)] + [(r, 0) for r in range(1, nz)] + [(0, 0)]
-    for r, c in order:
+    for count, (r, c) in enumerate(order):
+        for work in between.get(count, ()):
+            work()
         zt, xt = near(r, c)
         value = term(at(zt, xt))
         fresh = []

time: 103 us -> 106 us (1.029)
  Pallas kernels: 103 us -> 105 us
    pallas_call x1, Pallas kernels: 100 us -> 103 us  [attention(): pl.pallas_call(lambda *refs: kernel_body(heads, wide, *refs), out_shape=(...]
where the time goes in v8:
time: 106 us
  Pallas kernels  105 us (99%)
    pallas_call x1, Pallas kernels, attention(): pl.pallas_call(lambda *refs: kernel_body(heads, wide, *refs), out_shape=(...  103 us
    pallas_call x1, Pallas kernels, finish(): pl.pallas_call(lambda *refs: finish_body(heads, *refs), out_shape=(grad,...  2.27 us

profile of v8, /device:TPU:0, one launch (start us, length us, event | category | flops | bytes accessed | tf_op | source)
XLA Modules:
  0.0 106.1 jit_solution(870563391326978065)
XLA Ops:
  0.6 103.2 %attention.1 = (bf16[512,256]{1,0:T(8,128)(2,1)}, bf16[4,2,256,128]{3,2,1,0:T(8,128)(2,1)}, f32[256,256]{1,0:T(8,128)}) custom-call(bf16[512,256]{1,0:T(8,128)(2,1)} %refs_0_.1, bf16[512,256]{1,0:T(8,128)(2,1)} %refs_1_.1, bf16[512,256]{1,0:T(8,128)(2,1)} %refs_2_.1, bf16[512,256]{1,0:T(8,128)(2,1)} %refs_3_.1, f32[2,512]{1,0:T(2,128)} %bitcast.1, ...), custom_call_target="tpu_custom_call" | custom-call | flops 21474836480 | bytes 4194304 | tf_op jit(solution)/shard_map/attention/pallas_call | solution.py:730
  103.9 2.3 %finish.1 = (f32[512,256]{1,0:T(8,128)}, f32[512,256]{1,0:T(8,128)}, f32[512,256]{1,0:T(8,128)}, f32[256,256]{1,0:T(8,128)}) custom-call(bf16[512,256]{1,0:T(8,128)(2,1)} %get-tuple-element.7.refs_0_, bf16[4,2,256,128]{3,2,1,0:T(8,128)(2,1)} %get-tuple-element.8.refs_1_, f32[256,256]{1,0:T(8,128)} %get-tuple-element.9.refs_2_), custom_call_target="tpu_custom_call" | custom-call | tf_op jit(solution)/shard_map/finish/pallas_call | solution.py:830

commit v9 on v8

--- a/solution.py
+++ b/solution.py
@@ -481,6 +481,10 @@
     def _(j):
         group(False, j)
 
+    @pl.loop(0, tiles // 2)
+    def _(t):
+        stat_copy(t).start()
+
     @pl.loop(tiles // 2, tiles)
     def _(j):
         pair_wait(j)
@@ -499,8 +503,6 @@
         def _(n):
             t = j + 1 + odd + 2 * n
             scores(j, (t, False), (t + 1, False))
-
-        stat_copy(j - tiles // 2).start()
 
         @pl.when(j < tiles - 1)
         def _():
@@ -540,10 +542,25 @@
     for tile in range(upper - 1, low_tiles - 1, -1):
         stage_parts(tile)
     second_sends(5)
-    for tile in range(low_tiles - 1, -1, -1):
+    for tile in range(upper - 1, -1, -1):
         first_sends(tile)
-    for tile in range(upper - 1, low_tiles - 1, -1):
-        first_sends(tile)
+    add_on_way(4)
+    reduce(7)
+    second_sends(4)
+    add_on_way(3)
+    fin_sends(7)
+    add_on_way(2)
+    second_sends(3)
+    reduce(6)
+    second_sends(2)
+    add_on_way(1)
+    fin_sends(6)
+    add_on_way(0)
+    second_sends(1)
+    reduce(5)
+    second_sends(0)
+    reduce(4)
+    fin_sends(5)
 
     for r in range(nz):
         for c in range(nx):
@@ -557,6 +574,7 @@
                 value = value + dq_got[h * halves + m, n].astype(jnp.float32)
             low[n * sub : (n + 1) * sub, h * HEAD : (h + 1) * HEAD] = value.astype(LOW)
     low_copy = pltpu.make_async_copy(low, low_out, out_sem.at[0])
+    fin_sends(4)
     for r in range(wide // 2):
         source = lax.rem(twin + 2 * r, wide)
         pltpu.make_async_remote_copy(
@@ -576,20 +594,9 @@
             go(copy)
         waiting.clear()
 
-    between = {
-        1: (lambda: add_on_way(4), lambda: reduce(7)),
-        3: (lambda: second_sends(4), lambda: fin_sends(7), lambda: add_on_way(1)),
-        5: (lambda: second_sends(1), lambda: reduce(6), lambda: add_on_way(0)),
-        7: (lambda: second_sends(0), lambda: fin_sends(6), lambda: add_on_way(3)),
-        9: (lambda: second_sends(3), lambda: reduce(5), lambda: add_on_way(2)),
-        11: (lambda: second_sends(2), lambda: fin_sends(5), lambda: reduce(4)),
-        13: (lambda: fin_sends(4),),
-    }
     order = [(r, c) for r in range(1, nz) for c in range(1, nx)]
     order += [(0, c) for c in range(1, nx)] + [(r, 0) for r in range(1, nz)] + [(0, 0)]
-    for count, (r, c) in enumerate(order):
-        for work in between.get(count, ()):
-            work()
+    for r, c in order:
         zt, xt = near(r, c)
         value = term(at(zt, xt))
         fresh = []

time: 106 us -> 103 us (0.972)
  Pallas kernels: 105 us -> 102 us
    pallas_call x1, Pallas kernels: 103 us -> 99.8 us  [attention(): pl.pallas_call(lambda *refs: kernel_body(heads, wide, *refs), out_shape=(...]
where the time goes in v9:
time: 103 us
  Pallas kernels  102 us (99%)
    pallas_call x1, Pallas kernels, attention(): pl.pallas_call(lambda *refs: kernel_body(heads, wide, *refs), out_shape=(...  99.8 us
    pallas_call x1, Pallas kernels, finish(): pl.pallas_call(lambda *refs: finish_body(heads, *refs), out_shape=(grad,...  2.27 us

profile of v9, /device:TPU:0, one launch (start us, length us, event | category | flops | bytes accessed | tf_op | source)
XLA Modules:
  0.0 102.7 jit_solution(4408158467524816291)
XLA Ops:
  0.6 99.8 %attention.1 = (bf16[512,256]{1,0:T(8,128)(2,1)}, bf16[4,2,256,128]{3,2,1,0:T(8,128)(2,1)}, f32[256,256]{1,0:T(8,128)}) custom-call(bf16[512,256]{1,0:T(8,128)(2,1)} %refs_0_.1, bf16[512,256]{1,0:T(8,128)(2,1)} %refs_1_.1, bf16[512,256]{1,0:T(8,128)(2,1)} %refs_2_.1, bf16[512,256]{1,0:T(8,128)(2,1)} %refs_3_.1, f32[2,512]{1,0:T(2,128)} %bitcast.1, ...), custom_call_target="tpu_custom_call" | custom-call | flops 21474836480 | bytes 4194304 | tf_op jit(solution)/shard_map/attention/pallas_call | solution.py:737
  100.4 2.3 %finish.1 = (f32[512,256]{1,0:T(8,128)}, f32[512,256]{1,0:T(8,128)}, f32[512,256]{1,0:T(8,128)}, f32[256,256]{1,0:T(8,128)}) custom-call(bf16[512,256]{1,0:T(8,128)(2,1)} %get-tuple-element.7.refs_0_, bf16[4,2,256,128]{3,2,1,0:T(8,128)(2,1)} %get-tuple-element.8.refs_1_, f32[256,256]{1,0:T(8,128)} %get-tuple-element.9.refs_2_), custom_call_target="tpu_custom_call" | custom-call | tf_op jit(solution)/shard_map/finish/pallas_call | solution.py:837

commit v10 on v9

--- a/solution.py
+++ b/solution.py
@@ -545,22 +545,17 @@
     for tile in range(upper - 1, -1, -1):
         first_sends(tile)
     add_on_way(4)
-    reduce(7)
+    add_on_way(3)
     second_sends(4)
-    add_on_way(3)
-    fin_sends(7)
     add_on_way(2)
     second_sends(3)
-    reduce(6)
+    add_on_way(1)
     second_sends(2)
-    add_on_way(1)
-    fin_sends(6)
     add_on_way(0)
     second_sends(1)
-    reduce(5)
+    reduce(7)
     second_sends(0)
-    reduce(4)
-    fin_sends(5)
+    fin_sends(7)
 
     for r in range(nz):
         for c in range(nx):
@@ -574,7 +569,6 @@
                 value = value + dq_got[h * halves + m, n].astype(jnp.float32)
             low[n * sub : (n + 1) * sub, h * HEAD : (h + 1) * HEAD] = value.astype(LOW)
     low_copy = pltpu.make_async_copy(low, low_out, out_sem.at[0])
-    fin_sends(4)
     for r in range(wide // 2):
         source = lax.rem(twin + 2 * r, wide)
         pltpu.make_async_remote_copy(
@@ -594,9 +588,18 @@
             go(copy)
         waiting.clear()
 
+    between = {
+        2: (lambda: reduce(6),),
+        5: (lambda: fin_sends(6), lambda: reduce(5)),
+        8: (lambda: fin_sends(5), lambda: reduce(4)),
+        11: (lambda: fin_sends(4), lambda: reduce(3)),
+        14: (lambda: fin_sends(3),),
+    }
     order = [(r, c) for r in range(1, nz) for c in range(1, nx)]
     order += [(0, c) for c in range(1, nx)] + [(r, 0) for r in range(1, nz)] + [(0, 0)]
-    for r, c in order:
+    for count, (r, c) in enumerate(order):
+        for work in between.get(count, ()):
+            work()
         zt, xt = near(r, c)
         value = term(at(zt, xt))
         fresh = []
@@ -619,13 +622,13 @@
     flush()
     low_copy.start()
 
-    @pl.loop(0, 4)
+    @pl.loop(0, 3)
     def _(n):
-        reduce(3 - n)
+        reduce(2 - n)
 
         @pl.when(n > 0)
         def _():
-            fin_sends(4 - n)
+            fin_sends(3 - n)
 
 
     for n in list(range(1, nz)) + [0]:

time: 103 us -> 103 us (level)
  no operation moved by 1% of the time
where the time goes in v10:
time: 103 us
  Pallas kernels  102 us (99%)
    pallas_call x1, Pallas kernels, attention(): pl.pallas_call(lambda *refs: kernel_body(heads, wide, *refs), out_shape=(...  99.7 us
    pallas_call x1, Pallas kernels, finish(): pl.pallas_call(lambda *refs: finish_body(heads, *refs), out_shape=(grad,...  2.27 us

profile of v10, /device:TPU:0, one launch (start us, length us, event | category | flops | bytes accessed | tf_op | source)
XLA Modules:
  0.0 102.7 jit_solution(18438510411395721993)
XLA Ops:
  0.6 99.7 %attention.1 = (bf16[512,256]{1,0:T(8,128)(2,1)}, bf16[4,2,256,128]{3,2,1,0:T(8,128)(2,1)}, f32[256,256]{1,0:T(8,128)}) custom-call(bf16[512,256]{1,0:T(8,128)(2,1)} %refs_0_.1, bf16[512,256]{1,0:T(8,128)(2,1)} %refs_1_.1, bf16[512,256]{1,0:T(8,128)(2,1)} %refs_2_.1, bf16[512,256]{1,0:T(8,128)(2,1)} %refs_3_.1, f32[2,512]{1,0:T(2,128)} %bitcast.1, ...), custom_call_target="tpu_custom_call" | custom-call | flops 21474836480 | bytes 4194304 | tf_op jit(solution)/shard_map/attention/pallas_call | solution.py:740
  100.4 2.3 %finish.1 = (f32[512,256]{1,0:T(8,128)}, f32[512,256]{1,0:T(8,128)}, f32[512,256]{1,0:T(8,128)}, f32[256,256]{1,0:T(8,128)}) custom-call(bf16[512,256]{1,0:T(8,128)(2,1)} %get-tuple-element.7.refs_0_, bf16[4,2,256,128]{3,2,1,0:T(8,128)(2,1)} %get-tuple-element.8.refs_1_, f32[256,256]{1,0:T(8,128)} %get-tuple-element.9.refs_2_), custom_call_target="tpu_custom_call" | custom-call | tf_op jit(solution)/shard_map/finish/pallas_call | solution.py:840

commit v11 on v10

--- a/solution.py
+++ b/solution.py
@@ -38,7 +38,7 @@
     sub = qg.shape[2]
     tiles = blocks // 2
     span = w_out.shape[0]
-    part_rows = span // 2
+    part_rows = wa_own.shape[1]
     x_width = x_hbm.shape[1]
     column = lax.axis_index("tp")
     me = lax.axis_index("sp")
@@ -736,7 +736,8 @@
     f32 = jnp.float32
     dma = pltpu.SemaphoreType.DMA
     span = x.shape[1] * wide // blocks
-    part = span // 2
+    part = span * 3 // 8
+    rest = span - part
     return pl.pallas_call(
         lambda *refs: kernel_body(heads, wide, *refs),
         out_shape=(
@@ -775,15 +776,15 @@
             pltpu.VMEM((wide, rows, x.shape[1]), LOW),
             pltpu.VMEM((rows, cols), LOW),
             pltpu.VMEM((nz, nx, part, cols), LOW),
-            pltpu.VMEM((nz, nx, part, cols), LOW),
+            pltpu.VMEM((nz, nx, rest, cols), LOW),
             pltpu.VMEM((nx, nz, part, cols), LOW),
-            pltpu.VMEM((nz, nx, part, cols), LOW),
+            pltpu.VMEM((nz, nx, rest, cols), LOW),
             pltpu.VMEM((nz, part, cols), f32),
-            pltpu.VMEM((nx, part, cols), f32),
+            pltpu.VMEM((nx, rest, cols), f32),
             pltpu.VMEM((nz, part, cols), LOW),
-            pltpu.VMEM((nx, part, cols), LOW),
+            pltpu.VMEM((nx, rest, cols), LOW),
             pltpu.VMEM((nz, part, cols), LOW),
-            pltpu.VMEM((nx, part, cols), LOW),
+            pltpu.VMEM((nx, rest, cols), LOW),
             dma((6,)), dma((3,)),
             dma((blocks, 2)), dma((nz, 2, 2)), dma((nz, 2)), dma((nz, 2)), dma((blocks, 2)), dma((heads, nx, 2)),
             dma((heads, nx, 2)), dma((nz, nx)), dma((blocks,)), dma((6,)),

time: 103 us -> 104 us (level)
  no operation moved by 1% of the time
where the time goes in v11:
time: 104 us; the launch traced here: 103 us
  Pallas kernels  103 us (99%)
    pallas_call x1, Pallas kernels, attention(): pl.pallas_call(lambda *refs: kernel_body(heads, wide, *refs), out_shape=(...  101 us
    pallas_call x1, Pallas kernels, finish(): pl.pallas_call(lambda *refs: finish_body(heads, *refs), out_shape=(grad,...  2.27 us

profile of v11, /device:TPU:0, one launch (start us, length us, event | category | flops | bytes accessed | tf_op | source)
XLA Modules:
  0.0 103.4 jit_solution(1952518672954528274)
XLA Ops:
  0.6 100.5 %attention.1 = (bf16[512,256]{1,0:T(8,128)(2,1)}, bf16[4,2,256,128]{3,2,1,0:T(8,128)(2,1)}, f32[256,256]{1,0:T(8,128)}) custom-call(bf16[512,256]{1,0:T(8,128)(2,1)} %refs_0_.1, bf16[512,256]{1,0:T(8,128)(2,1)} %refs_1_.1, bf16[512,256]{1,0:T(8,128)(2,1)} %refs_2_.1, bf16[512,256]{1,0:T(8,128)(2,1)} %refs_3_.1, f32[2,512]{1,0:T(2,128)} %bitcast.1, ...), custom_call_target="tpu_custom_call" | custom-call | flops 21474836480 | bytes 4194304 | tf_op jit(solution)/shard_map/attention/pallas_call | solution.py:741
  101.2 2.3 %finish.1 = (f32[512,256]{1,0:T(8,128)}, f32[512,256]{1,0:T(8,128)}, f32[512,256]{1,0:T(8,128)}, f32[256,256]{1,0:T(8,128)}) custom-call(bf16[512,256]{1,0:T(8,128)(2,1)} %get-tuple-element.7.refs_0_, bf16[4,2,256,128]{3,2,1,0:T(8,128)(2,1)} %get-tuple-element.8.refs_1_, f32[256,256]{1,0:T(8,128)} %get-tuple-element.9.refs_2_), custom_call_target="tpu_custom_call" | custom-call | tf_op jit(solution)/shard_map/finish/pallas_call | solution.py:841

commit v12 on v11

--- a/solution.py
+++ b/solution.py
@@ -736,7 +736,7 @@
     f32 = jnp.float32
     dma = pltpu.SemaphoreType.DMA
     span = x.shape[1] * wide // blocks
-    part = span * 3 // 8
+    part = span * 5 // 8
     rest = span - part
     return pl.pallas_call(
         lambda *refs: kernel_body(heads, wide, *refs),

time: 104 us -> 105 us (level)
    pallas_call x1, Pallas kernels: 101 us -> 102 us  [attention(): pl.pallas_call(lambda *refs: kernel_body(heads, wide, *refs), out_shape=(...]
where the time goes in v12:
time: 105 us
  Pallas kernels  104 us (99%)
    pallas_call x1, Pallas kernels, attention(): pl.pallas_call(lambda *refs: kernel_body(heads, wide, *refs), out_shape=(...  102 us
    pallas_call x1, Pallas kernels, finish(): pl.pallas_call(lambda *refs: finish_body(heads, *refs), out_shape=(grad,...  2.27 us

profile of v12, /device:TPU:0, one launch (start us, length us, event | category | flops | bytes accessed | tf_op | source)
XLA Modules:
  0.0 104.9 jit_solution(14621304620680193061)
XLA Ops:
  0.6 102.0 %attention.1 = (bf16[512,256]{1,0:T(8,128)(2,1)}, bf16[4,2,256,128]{3,2,1,0:T(8,128)(2,1)}, f32[256,256]{1,0:T(8,128)}) custom-call(bf16[512,256]{1,0:T(8,128)(2,1)} %refs_0_.1, bf16[512,256]{1,0:T(8,128)(2,1)} %refs_1_.1, bf16[512,256]{1,0:T(8,128)(2,1)} %refs_2_.1, bf16[512,256]{1,0:T(8,128)(2,1)} %refs_3_.1, f32[2,512]{1,0:T(2,128)} %bitcast.1, ...), custom_call_target="tpu_custom_call" | custom-call | flops 21474836480 | bytes 4194304 | tf_op jit(solution)/shard_map/attention/pallas_call | solution.py:741
  102.7 2.3 %finish.1 = (f32[512,256]{1,0:T(8,128)}, f32[512,256]{1,0:T(8,128)}, f32[512,256]{1,0:T(8,128)}, f32[256,256]{1,0:T(8,128)}) custom-call(bf16[512,256]{1,0:T(8,128)(2,1)} %get-tuple-element.7.refs_0_, bf16[4,2,256,128]{3,2,1,0:T(8,128)(2,1)} %get-tuple-element.8.refs_1_, f32[256,256]{1,0:T(8,128)} %get-tuple-element.9.refs_2_), custom_call_target="tpu_custom_call" | custom-call | tf_op jit(solution)/shard_map/finish/pallas_call | solution.py:841
